TPU v7x, 32 devices: a whole 2x2x4 slice. The times are simulated.
32 devices in a mesh: grp: 2 (over y), sp: 16 (over z, x, core), tp: 1.
Axes of the slice: x: 2, y: 2, z: 4, core: 2. Of those that a mesh axis runs over, the one named last changes fastest.
Arguments:
- resid: bfloat16 [8192, 2048], P(('grp', 'sp', 'tp')), parts along dimension 0, may hold values from -6 to 6
- gate_b: bfloat16 [8192, 2048], P(('grp', 'sp'), 'tp'), parts along dimension 0, may hold values from -6 to 6
- gate_c: bfloat16 [8192, 2048], P(('grp', 'sp'), 'tp'), parts along dimension 0, may hold values from -6 to 6
- value: bfloat16 [8192, 2048], P(('grp', 'sp'), 'tp'), parts along dimension 0, may hold values from -6 to 6
- taps: bfloat16 [3, 2048], P(None, 'tp'), may hold values from -3.5 to 3.5
- doc_ids: int32 [8192], P(('grp', 'sp')), parts along dimension 0, may hold values from 0 to 3, never falling along the last dimension, each value on 1 to 2048 neighbouring positions
- out_weight: bfloat16 [2048, 2048], P('tp'), may hold values from -0.125 to 0.125
- norm_gains: float32 [3, 2048], replicated, may hold values from 0.1 to 1.9
- routes: int32 [8192, 2], P(('grp', 'sp')), parts along dimension 0, may hold values from 0 to 15, all different within a row; in each aligned block of 256 rows (0 to 255, 256 to 511, ...) at most 48 rows name the same one
- route_weights: float32 [8192, 2], P(('grp', 'sp')), parts along dimension 0, may hold values from 0.2 to 1
- w_gate: bfloat16 [16, 2048, 4096], P('sp', None, 'tp'), may hold values from -0.125 to 0.125
- w_up: bfloat16 [16, 2048, 4096], P('sp', None, 'tp'), may hold values from -0.125 to 0.125
- w_down: bfloat16 [16, 4096, 2048], P('sp', 'tp'), may hold values from -0.09375 to 0.09375
Outputs:
- layer_out: bfloat16 [8192, 2048], P(('grp', 'sp', 'tp')), parts along dimension 0
There are 2 independent parts, one for each index of `grp`. A program takes and returns all parts, laid end to end along the dimension named above; an argument that names none is the same for every part. Nothing has to cross between parts.
Inputs may be any that keep to these rules, and one draw needn't show every extreme that they name: `doc_ids`: never falling along the sequence; each document spans 1 to 2048 positions. `routes`: each row names 2 different experts. In each aligned block of 256 rows no expert is named more than 48 times, and in every draw some block names some expert exactly 48 times.
All inputs are finite; a program needn't handle non-finite values.
Results may differ from a plain program's by a relative error of at most 0.02.
Values may be sent and summed in bfloat16 or wider, within the bound.
No kernel may reach another device: no remote copies, remote signals or barrier semaphores. Data moves between devices by JAX's collectives and lax.ppermute only.
A program may use at most 128 MiB of HBM per device.

v0:
```python
import jax
import jax.numpy as jnp
from jax import lax
from jax.sharding import PartitionSpec as P

TAPS = 3
TOP = 2


norm_eps = 1e-06


def passed_along(block, axis, distance):
    devices = range(lax.axis_size(axis))
    route = [(i - distance, i) for i in devices if i - distance in devices]
    return lax.ppermute(block, axis, route)


def rms_scale(values, gain_row):
    mean_sq = jnp.mean(values * values, axis=-1, keepdims=True)
    return values * lax.rsqrt(mean_sq + norm_eps) * gain_row


def slot_table(block_routes, experts, capacity):
    block_count = block_routes.shape[0]
    block_len = block_routes.shape[1]
    flat_routes = block_routes.reshape(block_count, block_len * TOP)
    onehot = (
        flat_routes[:, :, None] == jnp.arange(experts, dtype=jnp.int32)[None, None, :]
    ).astype(jnp.int32)
    before = jnp.cumsum(onehot, axis=1) - onehot
    slot_rank = jnp.sum(before * onehot, axis=2)
    slot_hit = onehot[:, :, :, None] * (
        slot_rank[:, :, None, None] == jnp.arange(capacity, dtype=jnp.int32)[None, None, None, :]
    ).astype(jnp.int32)
    owner_row = jnp.arange(block_len * TOP, dtype=jnp.int32) // TOP
    slot_tok = jnp.sum(slot_hit * owner_row[None, :, None, None], axis=1)
    filled = jnp.sum(slot_hit, axis=1)
    return (slot_rank.reshape(block_count, block_len, TOP), slot_tok, filled)


def pick_rows(normed_rows, slot_tok, filled):
    picked_rows = normed_rows[slot_tok]
    return jnp.where(filled[:, :, None] > 0, picked_rows, jnp.zeros_like(picked_rows))


def expert_hidden(picked_rows, w_gate, w_up):
    gate_proj = jnp.dot(picked_rows, w_gate[0], preferred_element_type=jnp.float32)
    up_proj = jnp.dot(picked_rows, w_up[0], preferred_element_type=jnp.float32)
    return (jax.nn.silu(gate_proj) * up_proj).astype(jnp.bfloat16)


def per_device(
    resid,
    gate_b,
    gate_c,
    value,
    taps,
    doc_ids,
    out_weight,
    norm_gains,
    routes,
    route_weights,
    w_gate,
    w_up,
    w_down,
):
    tok_dev = gate_b.shape[0]
    rows_blk = resid.shape[0]
    model_width = resid.shape[1]
    experts = lax.axis_size("sp")
    capacity = max(2, 3 * TOP * rows_blk // (2 * experts))
    tap_reach = TAPS - 1
    product = gate_c.astype(jnp.float32) * value.astype(jnp.float32)
    id_values = doc_ids.astype(jnp.float32)
    prev_rows, prev_ids = passed_along(
        (product[tok_dev - tap_reach :], id_values[tok_dev - tap_reach :]), "sp", 1
    )
    ext_rows = jnp.concatenate([prev_rows, product], axis=0)
    ext_ids = jnp.concatenate([prev_ids, id_values], axis=0)
    tap_weights = taps.astype(jnp.float32)
    convolved = tap_weights[0] * product
    for distance in range(1, TAPS):
        earlier = ext_rows[tap_reach - distance : tap_reach - distance + tok_dev]
        same_doc = ext_ids[tap_reach - distance : tap_reach - distance + tok_dev] == id_values
        convolved = convolved + jnp.where(same_doc[:, None], tap_weights[distance] * earlier, 0.0)
    mixed_rows = (gate_b.astype(jnp.float32) * convolved).astype(jnp.bfloat16)
    block_rows = mixed_rows
    projected = lax.psum_scatter(
        jnp.dot(block_rows, out_weight, preferred_element_type=jnp.float32).astype(jnp.bfloat16),
        "tp",
        scatter_dimension=0,
        tiled=True,
    ).astype(jnp.float32)
    stream = resid.astype(jnp.float32) + rms_scale(projected, norm_gains[0])
    normed = rms_scale(stream, norm_gains[1]).astype(jnp.bfloat16)
    lane_index = lax.axis_index("tp")
    offset = lane_index * rows_blk
    my_routes = lax.dynamic_slice_in_dim(routes, offset, rows_blk, 0)
    my_weights = lax.dynamic_slice_in_dim(route_weights, offset, rows_blk, 0)
    own_rank, own_tok, own_filled = slot_table(my_routes[None], experts, capacity)
    slot_rank = own_rank[0]
    outgoing = pick_rows(normed, own_tok[0], own_filled[0])
    arrived = lax.all_to_all(outgoing, "sp", split_axis=0, concat_axis=0, tiled=True)
    hidden = expert_hidden(
        lax.all_gather(arrived[None], "tp", axis=0, tiled=True).reshape(-1, model_width),
        w_gate,
        w_up,
    )
    block_rows = hidden
    summed = lax.psum_scatter(
        jnp.dot(block_rows, w_down[0], preferred_element_type=jnp.float32).astype(jnp.bfloat16),
        "tp",
        scatter_dimension=0,
        tiled=True,
    )
    results = summed.reshape(experts, capacity, model_width)
    returned = lax.all_to_all(results, "sp", split_axis=0, concat_axis=0, tiled=True)
    picked = returned[my_routes, slot_rank]
    shares = my_weights / jnp.sum(my_weights, axis=1, keepdims=True)
    combined = jnp.sum(shares[:, :, None] * picked.astype(jnp.float32), axis=1)
    return (stream + rms_scale(combined, norm_gains[2])).astype(jnp.bfloat16)


def solution(mesh):
    return jax.shard_map(
        per_device,
        mesh=mesh,
        in_specs=(
            P(("grp", "sp", "tp"), None),
            P(("grp", "sp"), "tp"),
            P(("grp", "sp"), "tp"),
            P(("grp", "sp"), "tp"),
            P(None, "tp"),
            P(("grp", "sp")),
            P("tp", None),
            P(),
            P(("grp", "sp"), None),
            P(("grp", "sp"), None),
            P("sp", None, "tp"),
            P("sp", None, "tp"),
            P("sp", "tp", None),
        ),
        out_specs=P(("grp", "sp", "tp"), None),
        check_vma=False,
    )
```

profile of v0, /device:TPU:11, one launch (start us, length us, event | category | flops | bytes accessed | tf_op | source)
XLA Modules:
  0.0 265.3 jit_solution(12587690889693497333)
XLA Ops:
  0.0 0.7 convert_element_type.72
  0.8 3.9 %collective-permute-start = (f32[2]{0:T(128)S(1)}, f32[2]{0:T(128)S(1)}, u32[]{:S(2)}, u32[]{:S(2)}) collective-permute-start(f32[2]{0:T(128)S(1)} %slice.43), channel_id=1, source_target_pairs={{0,1},{1,2},{2,3},{3,4},{4,5},{5,6},{6,7},{7,8},{8,9},{9,10},{10,1... | collective-permute-start | bytes 32 | tf_op jit(solution)/shard_map/ppermute | solution.py:16
  4.6 1.9 convert_multiply_fusion.2
  6.6 1.9 collective-permute-start.1
  8.5 0.1 copy.36
  8.6 0.1 eq.63
  8.8 1.2 reduce-window.6
  10.0 0.2 slice_reduce_fusion
  10.4 0.1 copy.39
  10.6 0.6 multiply_reduce_fusion.1
  11.6 6.8 %fusion.23 = (f32[256]{0:T(256)S(1)}, bf16[256,2048]{1,0:T(8,128)(2,1)S(1)}) fusion(bf16[2048,2048]{1,0:T(8,128)(2,1)} %param.19, f32[2,2048]{1,0:T(2,128)S(1)} %collective-permute-done.1, f32[256,2048]{1,0:T(8,128)S(1)} %convert_multiply_fusion.2, bf16[256,2048]{1,0:T(8,128)(2,1)} %param.14, f32[2048]{0:T(1024)S(1)} %bitcast.68, f32[2048]{0:T(1024)S(1)} %bitcast.67, ...), kind=kOutput, calls=%fused_computation.27 | convolution fusion | flops 2155872000 | bytes 12625408 | tf_op jit(solution)/shard_map/dot_general | solution.py:90
  18.4 0.6 multiply_reduce_fusion.3
  19.0 0.3 copy-done.2
  19.3 0.6 multiply_convert_fusion.1
  20.0 4.3 %gather_fusion = bf16[768,2048]{1,0:T(8,128)(2,1)} fusion(bf16[256,2048]{1,0:T(8,128)(2,1)S(1)} %multiply_convert_fusion.1, s32[1024]{0:T(1024)S(1)} %pad_clamp_fusion), kind=kCustom, calls=%fused_computation | custom fusion | bytes 6294528 | tf_op jit(solution)/shard_map/gather | solution.py:43
  24.2 2.2 broadcast_select_fusion
  26.4 74.9 %all_to_all.10 = bf16[16,48,2048]{2,1,0:T(8,128)(2,1)S(1)} all-to-all(bf16[16,48,2048]{2,1,0:T(8,128)(2,1)S(1)} %broadcast_select_fusion), channel_id=1, replica_groups=mesh['grp'=2,'sp'=16,'tp'=1] {'sp'}, dimensions={0} | all-to-all | bytes 6291456 | tf_op jit(solution)/shard_map/all_to_all | solution.py:104
  101.3 19.3 %fusion.4 = f32[768,4096]{1,0:T(8,128)} fusion(bf16[768,2048]{1,0:T(8,128)(2,1)S(1)} %bitcast.55, bf16[1,2048,4096]{2,1,0:T(8,128)(2,1)} %param.23), kind=kOutput, calls=%fused_computation.6 | convolution fusion | flops 12884901888 | bytes 32505856 | tf_op jit(solution)/shard_map/dot_general | solution.py:48
  120.7 40.4 %fusion.11 = bf16[768,2048]{1,0:T(8,128)(2,1)} fusion(bf16[1,4096,2048]{2,1,0:T(8,128)(2,1)} %param.25, f32[768,4096]{1,0:T(8,128)} %fusion.4, bf16[768,2048]{1,0:T(8,128)(2,1)S(1)} %bitcast.56, bf16[1,2048,4096]{2,1,0:T(8,128)(2,1)} %param.24), kind=kOutput, calls=%fused_computation.11 | convolution fusion | flops 25790251008 | bytes 52428800 | tf_op jit(solution)/shard_map/dot_general | solution.py:112
  161.1 5.2 %all-to-all-start.1 = ((bf16[16,48,2048]{2,1,0:T(8,128)(2,1)}), bf16[16,48,2048]{2,1,0:T(8,128)(2,1)S(1)}, u32[]{:S(2)}, u32[]{:S(2)}) async-start(bf16[16,48,2048]{2,1,0:T(8,128)(2,1)} %bitcast.54), calls=%async_computation.1 | async-start | bytes 6291456 | tf_op jit(solution)/shard_map/all_to_all | solution.py:118
  166.3 0.1 squeeze_reshape.3
  166.6 0.1 copy.43
  166.7 0.1 reshape.289
  166.9 0.1 copy.35
  167.1 69.2 %all-to-all-done.1 = bf16[16,48,2048]{2,1,0:T(8,128)(2,1)S(1)} async-done(((bf16[16,48,2048]{2,1,0:T(8,128)(2,1)}), bf16[16,48,2048]{2,1,0:T(8,128)(2,1)S(1)}, u32[]{:S(2)}, u32[]{:S(2)}) %all-to-all-start.1) | async-done | bytes 3145760 | tf_op jit(solution)/shard_map/all_to_all | solution.py:118
  236.2 11.5 %gather_fusion.1 = bf16[512,2048]{1,0:T(8,128)(2,1)} fusion(bf16[16,48,2048]{2,1,0:T(8,128)(2,1)S(1)} %all-to-all-done.1, s32[512]{0:T(512)S(1)} %reshape.289), kind=kCustom, calls=%fused_computation.1 | custom fusion | bytes 4198400 | tf_op jit(solution)/shard_map/gather | solution.py:119
  247.7 5.4 %reshape.296 = f32[256,2,2048]{2,1,0:T(2,128)} reshape(bf16[512,2048]{1,0:T(8,128)(2,1)} %gather_fusion.1) | data formatting | bytes 6291456 | tf_op jit(solution)/shard_map/convert_element_type | solution.py:121
  253.2 8.9 %multiply_reduce_fusion = f32[256,2048]{1,0:T(8,128)S(1)} fusion(f32[256,2,2048]{2,1,0:T(2,128)} %reshape.296, f32[256,2]{1,0:T(8,128)S(1)} %copy.35), kind=kLoop, calls=%fused_computation.10 | loop fusion | flops 1572864 | bytes 6293504 | tf_op jit(solution)/shard_map/reduce_sum | solution.py:121
  262.1 0.2 multiply_reduce_fusion.2
  262.3 1.0 copy-done.1
  263.3 0.3 copy-done.3
  263.6 1.7 add_convert_fusion
  (44 shorter events, 0.8 us)
Async XLA Ops:
  0.8 7.7 %copy-start.6 = (s32[256,2]{0,1:T(2,128)S(1)}, s32[256,2]{0,1:T(2,128)}, u32[]{:S(2)}) copy-start(s32[256,2]{0,1:T(2,128)} %param.21) | copy-start | bytes 6148
  0.8 9.5 %copy-start.4 = (bf16[3,2048]{1,0:T(4,128)(2,1)S(1)}, bf16[3,2048]{1,0:T(4,128)(2,1)}, u32[]{:S(2)}) copy-start(bf16[3,2048]{1,0:T(4,128)(2,1)} %param.17) | copy-start | bytes 36868
  0.8 9.5 %copy-start.5 = (f32[3,2048]{1,0:T(4,128)S(1)}, f32[3,2048]{1,0:T(4,128)}, u32[]{:S(2)}) copy-start(f32[3,2048]{1,0:T(4,128)} %param.20) | copy-start | bytes 73732
  0.8 10.7 %copy-start.8 = (s32[256]{0:T(256)S(1)}, s32[256]{0:T(256)}, u32[]{:S(2)}) copy-start(s32[256]{0:T(256)} %param.18) | copy-start | bytes 3076
  0.8 10.6 %collective-permute-start = (f32[2]{0:T(128)S(1)}, f32[2]{0:T(128)S(1)}, u32[]{:S(2)}, u32[]{:S(2)}) collective-permute-start(f32[2]{0:T(128)S(1)} %slice.43), channel_id=1, source_target_pairs={{0,1},{1,2},{2,3},{3,4},{4,5},{5,6},{6,7},{7,8},{8,9},{9,10},{10,1... | collective-permute-start | bytes 32 | tf_op jit(solution)/shard_map/ppermute | solution.py:16
  6.6 5.0 %collective-permute-start.1 = (f32[2,2048]{1,0:T(2,128)S(1)}, f32[2,2048]{1,0:T(2,128)S(1)}, u32[]{:S(2)}, u32[]{:S(2)}) collective-permute-start(f32[2,2048]{1,0:T(2,128)S(1)} %slice.62), channel_id=1, source_target_pairs={{0,1},{1,2},{2,3},{3,4},{4,5},{5,6},{6,7},{7,8},{8,9},{9,10},{10,1... | collective-permute-start | bytes 49160 | tf_op jit(solution)/shard_map/ppermute | solution.py:16
  11.6 6.8 %copy-start = (bf16[256,2048]{1,0:T(8,128)(2,1)S(1)}, bf16[256,2048]{1,0:T(8,128)(2,1)}, u32[]{:S(2)}) copy-start(bf16[256,2048]{1,0:T(8,128)(2,1)} %param.13) | copy-start | bytes 3145732
  18.3 1.0 copy-start.2
  161.1 5.8 %copy-start.7 = (f32[256,2]{0,1:T(2,128)S(1)}, f32[256,2]{0,1:T(2,128)}, u32[]{:S(2)}) copy-start(f32[256,2]{0,1:T(2,128)} %param.22) | copy-start | bytes 6148
  161.1 75.1 %all-to-all-start.1 = ((bf16[16,48,2048]{2,1,0:T(8,128)(2,1)}), bf16[16,48,2048]{2,1,0:T(8,128)(2,1)S(1)}, u32[]{:S(2)}, u32[]{:S(2)}) async-start(bf16[16,48,2048]{2,1,0:T(8,128)(2,1)} %bitcast.54), calls=%async_computation.1 | async-start | bytes 6291456 | tf_op jit(solution)/shard_map/all_to_all | solution.py:118
  262.1 1.2 copy-start.1
  262.1 1.5 copy-start.3
where the time goes:
time: 266 us; the launch traced here: 265 us
  blocking collectives  74.9 us (28%)
  waiting for transfers between devices  69.2 us (26%)
  matrix products  66.6 us (25%)
  local copies, waits for them, and re-layouts  24.3 us (9%)
  other arithmetic  19 us (7%)
  starting transfers between devices  11 us (4%)
    all_to_all x1, blocking collectives, per_device(): lax.all_to_all(outgoing, 'sp', split_axis=0, concat_axis=0, tiled=True)  74.9 us
    all_to_all x1, waiting for transfers between devices, per_device(): lax.all_to_all(results, 'sp', split_axis=0, concat_axis=0, tiled=True)  69.2 us
    dot_general x1, matrix products, per_device(): jnp.dot(block_rows, w_down[0], preferred_element_type=jnp.float32)  40.4 us
    dot_general x1, matrix products, expert_hidden(): jnp.dot(picked_rows, w_gate[0], preferred_element_type=jnp.float32)  19.3 us
    gather x1, local copies, waits for them, and re-layouts, per_device(): picked = returned[my_routes, slot_rank]  11.5 us
    reduce_sum x1, other arithmetic, per_device(): combined = jnp.sum(shares[:, :, None] * picked.astype(jnp.float32), axis=1)  8.89 us
    dot_general x1, matrix products, per_device(): jnp.dot(block_rows, out_weight, preferred_element_type=jnp.float32)  6.79 us
    ppermute x2, starting transfers between devices, passed_along(): return lax.ppermute(block, axis, route)  5.78 us
  transfers between devices with their start and end apart: 3, of which 1 were waited for; matrix products, arithmetic and copies ran while one was open for 2% of the time, Pallas kernels for 0%

commit v1 on v0

v1 whole, which is shorter than its diff:
```python
import math

import jax
import jax.numpy as jnp
from jax import lax
from jax.experimental import pallas as pl
from jax.experimental.pallas import tpu as pltpu
from jax.sharding import PartitionSpec as P


TAPS = 3
TOP = 2
CHUNKS = 2

norm_eps = 1e-06


def passed_along(block, axis, distance):
    devices = range(lax.axis_size(axis))
    route = [(i - distance, i) for i in devices if i - distance in devices]
    return lax.ppermute(block, axis, route)


def rms_scale(values, gain_row):
    mean_sq = jnp.mean(values * values, axis=-1, keepdims=True)
    return values * lax.rsqrt(mean_sq + norm_eps) * gain_row


def dot_f32(a, b, dims):
    return lax.dot_general(a, b, (dims, ((), ())), preferred_element_type=jnp.float32)


def route_tables(my_routes, my_weights, experts):
    rows = my_routes.shape[0]
    expert_ids = lax.broadcasted_iota(jnp.int32, (rows, experts), 1)
    shares = my_weights / jnp.sum(my_weights, axis=1, keepdims=True)
    named = jnp.zeros((rows, experts), jnp.bool_)
    share_of = jnp.zeros((rows, experts), jnp.float32)
    for k in range(TOP):
        hit = my_routes[:, k : k + 1] == expert_ids
        named = named | hit
        share_of = share_of + jnp.where(hit, shares[:, k : k + 1], 0.0)
    earlier = (
        lax.broadcasted_iota(jnp.int32, (rows, rows), 0)
        > lax.broadcasted_iota(jnp.int32, (rows, rows), 1)
    ).astype(jnp.bfloat16)
    before = dot_f32(earlier, named.astype(jnp.bfloat16), ((1,), (0,)))
    slot_of = jnp.where(named, before, -1.0).astype(jnp.bfloat16)
    high = lax.reduce_precision(share_of, 8, 7)
    return slot_of, high.astype(jnp.bfloat16), (share_of - high).astype(jnp.bfloat16)


def chunk_tables(tables, experts, first, size):
    slot_of, high, low = tables
    cols = lax.broadcasted_iota(jnp.int32, (experts, experts * size), 1)
    owner = lax.broadcasted_iota(jnp.int32, (experts, experts * size), 0)
    spread = (cols // size == owner).astype(jnp.bfloat16)
    col_slot = (lax.broadcasted_iota(jnp.int32, (1, experts * size), 1) % size + first).astype(jnp.float32)
    taken = dot_f32(slot_of, spread, ((1,), (0,))) == col_slot
    onehot = taken.astype(jnp.bfloat16)
    w_high = jnp.where(taken, dot_f32(high, spread, ((1,), (0,))), 0.0).astype(jnp.bfloat16)
    w_low = jnp.where(taken, dot_f32(low, spread, ((1,), (0,))), 0.0).astype(jnp.bfloat16)
    return onehot, w_high, w_low


def expert_body(rows_ref, gate_ref, up_ref, down_ref, out_ref, acc_ref):
    step = pl.program_id(0)
    rows = rows_ref[...]
    gate_proj = jnp.dot(rows, gate_ref[0], preferred_element_type=jnp.float32)
    up_proj = jnp.dot(rows, up_ref[0], preferred_element_type=jnp.float32)
    hidden = (gate_proj / (1.0 + jnp.exp(-gate_proj)) * up_proj).astype(jnp.bfloat16)
    part = jnp.dot(hidden, down_ref[0], preferred_element_type=jnp.float32)

    @pl.when(step == 0)
    def _():
        acc_ref[...] = part

    @pl.when(step > 0)
    def _():
        acc_ref[...] += part

    @pl.when(step == pl.num_programs(0) - 1)
    def _():
        out_ref[...] = acc_ref[...].astype(out_ref.dtype)


def expert_block(rows, w_gate, w_up, w_down):
    count, width = rows.shape
    units = w_gate.shape[2]
    block = math.gcd(units, 512)
    return pl.pallas_call(
        expert_body,
        grid=(units // block,),
        in_specs=[
            pl.BlockSpec((count, width), lambda j: (0, 0)),
            pl.BlockSpec((1, width, block), lambda j: (0, 0, j)),
            pl.BlockSpec((1, width, block), lambda j: (0, 0, j)),
            pl.BlockSpec((1, block, width), lambda j: (0, j, 0)),
        ],
        out_specs=pl.BlockSpec((count, width), lambda j: (0, 0)),
        out_shape=jax.ShapeDtypeStruct((count, width), jnp.bfloat16),
        scratch_shapes=[pltpu.VMEM((count, width), jnp.float32)],
        cost_estimate=pl.CostEstimate(
            flops=6 * count * width * units,
            transcendentals=count * units,
            bytes_accessed=6 * width * units + 4 * count * width,
        ),
        compiler_params=pltpu.CompilerParams(
            dimension_semantics=("arbitrary",), vmem_limit_bytes=48 * 2**20
        ),
        name="experts",
    )(rows, w_gate, w_up, w_down)


def mixer_rows(gate_b, gate_c, value, taps, doc_ids):
    tok_dev, width = gate_b.shape
    tap_reach = TAPS - 1
    ids_bf = jnp.broadcast_to(doc_ids[tok_dev - tap_reach :, None], (tap_reach, 128)).astype(jnp.bfloat16)
    packed = jnp.concatenate([gate_c[tok_dev - tap_reach :], value[tok_dev - tap_reach :], ids_bf], axis=1)
    got = passed_along(packed, "sp", 1).astype(jnp.float32)
    prev_rows = got[:, :width] * got[:, width : 2 * width]
    id_values = doc_ids.astype(jnp.float32)
    ext_ids = jnp.concatenate([got[:, 2 * width], id_values], axis=0)
    product = gate_c.astype(jnp.float32) * value.astype(jnp.float32)
    ext_rows = jnp.concatenate([prev_rows, product], axis=0)
    tap_weights = taps.astype(jnp.float32)
    convolved = tap_weights[0] * product
    for distance in range(1, TAPS):
        earlier = ext_rows[tap_reach - distance : tap_reach - distance + tok_dev]
        same_doc = ext_ids[tap_reach - distance : tap_reach - distance + tok_dev] == id_values
        convolved = convolved + jnp.where(same_doc[:, None], tap_weights[distance] * earlier, 0.0)
    return (gate_b.astype(jnp.float32) * convolved).astype(jnp.bfloat16)


def per_device(
    resid,
    gate_b,
    gate_c,
    value,
    taps,
    doc_ids,
    out_weight,
    norm_gains,
    routes,
    route_weights,
    w_gate,
    w_up,
    w_down,
):
    rows_blk = resid.shape[0]
    width = resid.shape[1]
    experts = lax.axis_size("sp")
    capacity = max(2, 3 * TOP * rows_blk // (2 * experts))
    offset = lax.axis_index("tp") * rows_blk
    my_routes = lax.dynamic_slice_in_dim(routes, offset, rows_blk, 0)
    my_weights = lax.dynamic_slice_in_dim(route_weights, offset, rows_blk, 0)
    tables = route_tables(my_routes, my_weights, experts)
    edges = [capacity * c // CHUNKS for c in range(CHUNKS + 1)]
    chunks = [chunk_tables(tables, experts, a, b - a) for a, b in zip(edges, edges[1:])]

    mixed = mixer_rows(gate_b, gate_c, value, taps, doc_ids)
    projected = lax.psum_scatter(
        jnp.dot(mixed, out_weight, preferred_element_type=jnp.float32).astype(jnp.bfloat16),
        "tp",
        scatter_dimension=0,
        tiled=True,
    ).astype(jnp.float32)
    stream = resid.astype(jnp.float32) + rms_scale(projected, norm_gains[0])
    normed = rms_scale(stream, norm_gains[1]).astype(jnp.bfloat16)

    combined = 0.0
    for (onehot, w_high, w_low), first, last in zip(chunks, edges, edges[1:]):
        size = last - first
        outgoing = dot_f32(onehot, normed, ((0,), (0,))).astype(jnp.bfloat16)
        arrived = lax.all_to_all(outgoing.reshape(experts, size, width), "sp", split_axis=0, concat_axis=0, tiled=True)
        rows = lax.all_gather(arrived[None], "tp", axis=0, tiled=True).reshape(-1, width)
        worked = expert_block(rows, w_gate, w_up, w_down)
        result = lax.psum_scatter(worked, "tp", scatter_dimension=0, tiled=True).reshape(experts, size, width)
        returned = lax.all_to_all(result, "sp", split_axis=0, concat_axis=0, tiled=True).reshape(-1, width)
        combined = combined + dot_f32(w_high, returned, ((1,), (0,))) + dot_f32(w_low, returned, ((1,), (0,)))
    return (stream + rms_scale(combined, norm_gains[2])).astype(jnp.bfloat16)


def solution(mesh):
    return jax.shard_map(
        per_device,
        mesh=mesh,
        in_specs=(
            P(("grp", "sp", "tp"), None),
            P(("grp", "sp"), "tp"),
            P(("grp", "sp"), "tp"),
            P(("grp", "sp"), "tp"),
            P(None, "tp"),
            P(("grp", "sp")),
            P("tp", None),
            P(),
            P(("grp", "sp"), None),
            P(("grp", "sp"), None),
            P("sp", None, "tp"),
            P("sp", None, "tp"),
            P("sp", "tp", None),
        ),
        out_specs=P(("grp", "sp", "tp"), None),
        check_vma=False,
    )
```

time: 266 us -> 194 us (0.73)
  blocking collectives: 74.9 us -> 0 us
  Pallas kernels: 0 us -> 55 us
  matrix products: 66.6 us -> 22.4 us
  local copies, waits for them, and re-layouts: 24.3 us -> 5.56 us
  other arithmetic: 19 us -> 6.61 us
  starting transfers between devices: 11 us -> 23.2 us
  waiting for transfers between devices: 69.2 us -> 80.2 us
    all_to_all x1 -> x0, blocking collectives: 74.9 us -> none  [per_device(): lax.all_to_all(outgoing, 'sp', split_axis=0, concat_axis=0, tiled=True)]
    pallas_call x0 -> x2, Pallas kernels: none -> 55 us  [expert_block(): pl.pallas_call(expert_body, grid=(units // block,), in_specs=[pl.BlockSpe...]
    dot_general x3 -> x10, matrix products: 66.6 us -> 22.4 us  [the longest x9 14 us: dot_f32(): lax.dot_general(a, b, (dims, ((), ())), preferred_element_type=jnp.float32)]
    gather x2 -> x0, local copies, waits for them, and re-layouts: 15.8 us -> none  [the longest x1 11.5 us: per_device(): picked = returned[my_routes, slot_rank]]
    all_to_all x1 -> x4, starting transfers between devices: 5.24 us -> 19.5 us  [the longest x2 9.76 us: per_device(): lax.all_to_all(outgoing.reshape(experts, size, width), 'sp', split_axis=0...]
    all_to_all x1 -> x4, waiting for transfers between devices: 69.2 us -> 80.2 us  [the longest x2 41 us: per_device(): lax.all_to_all(outgoing.reshape(experts, size, width), 'sp', split_axis=0...]
    reduce_sum x4 -> x1, other arithmetic: 9.63 us -> 0.02 us  [route_tables(): shares = my_weights / jnp.sum(my_weights, axis=1, keepdims=True)]
    convert_element_type x1 -> x0, local copies, waits for them, and re-layouts: 5.44 us -> none  [per_device(): combined = jnp.sum(shares[:, :, None] * picked.astype(jnp.float32), axis=1)]
  transfers between devices with their start and end apart: 3 -> 5, of which waited for: 1 -> 4; matrix products, arithmetic and copies ran while one was open for 2% -> 6% of each run, Pallas kernels for 0% -> 28%
where the time goes in v1:
time: 194 us; the launch traced here: 193 us
  waiting for transfers between devices  80.2 us (41%)
  Pallas kernels  55 us (28%)
  starting transfers between devices  23.2 us (12%)
  matrix products  22.4 us (12%)
  other arithmetic  6.61 us (3%)
  local copies, waits for them, and re-layouts  5.56 us (3%)
    pallas_call x2, Pallas kernels, expert_block(): pl.pallas_call(expert_body, grid=(units // block,), in_specs=[pl.BlockSpe...  55 us
    all_to_all x2, waiting for transfers between devices, per_device(): lax.all_to_all(outgoing.reshape(experts, size, width), 'sp', split_axis=0...  41 us
    all_to_all x2, waiting for transfers between devices, per_device(): lax.all_to_all(result, 'sp', split_axis=0, concat_axis=0, tiled=True)  39.2 us
    dot_general x9, matrix products, dot_f32(): lax.dot_general(a, b, (dims, ((), ())), preferred_element_type=jnp.float32)  14 us
    all_to_all x2, starting transfers between devices, per_device(): lax.all_to_all(outgoing.reshape(experts, size, width), 'sp', split_axis=0...  9.76 us
    all_to_all x2, starting transfers between devices, per_device(): lax.all_to_all(result, 'sp', split_axis=0, concat_axis=0, tiled=True)  9.74 us
    dot_general x1, matrix products, per_device(): jnp.dot(mixed, out_weight, preferred_element_type=jnp.float32)  8.42 us
  transfers between devices with their start and end apart: 5, of which 4 were waited for; matrix products, arithmetic and copies ran while one was open for 6% of the time, Pallas kernels for 28%

profile of v1, /device:TPU:11, one launch (start us, length us, event | category | flops | bytes accessed | tf_op | source)
XLA Modules:
  0.0 193.3 jit_solution(13233839838226321056)
XLA Ops:
  0.0 0.8 fusion.78
  0.8 0.8 slice.63
  1.6 0.8 slice.62
  2.5 3.7 %collective-permute-start = (bf16[2,4224]{1,0:T(2,128)(2,1)S(1)}, bf16[2,4224]{1,0:T(2,128)(2,1)S(1)}, u32[]{:S(2)}, u32[]{:S(2)}) collective-permute-start(bf16[2,4224]{1,0:T(2,128)(2,1)S(1)} %pad_maximum_fusion.1), channel_id=1, source_target_pairs={{0,1},{1,2},{2,3},{3,4},{4,5},{5,6},{6,7},{7,8},{8,9},{9,10},{10,1... | collective-permute-start | bytes 50696 | tf_op jit(solution)/shard_map/ppermute | solution.py:21
  6.3 3.3 %convert_multiply_fusion.2 = f32[256,2048]{1,0:T(8,128)} fusion(bf16[256,2048]{1,0:T(8,128)(2,1)} %param.16, bf16[256,2048]{1,0:T(8,128)(2,1)} %param.15), kind=kLoop, calls=%fused_computation.27 | loop fusion | flops 1572864 | bytes 4194304 | tf_op jit(solution)/shard_map/mul | solution.py:124
  9.7 0.5 broadcast_compare_fusion
  10.5 0.3 copy-done.12
  10.8 8.4 %fusion.7 = (f32[256]{0:T(256)S(1)}, bf16[256,2048]{1,0:T(8,128)(2,1)S(1)}) fusion(bf16[2048,2048]{1,0:T(8,128)(2,1)} %param.19, f32[2,2048]{1,0:T(2,128)S(1)} %slice_multiply_fusion, f32[256,2048]{1,0:T(8,128)} %convert_multiply_fusion.2, bf16[256,2048]{1,0:T(8,128)(2,1)S(1)} %copy-done.12, f32[2048]{0:T(1024)S(1)} %bitcast.43, f32[2048]{0:T(1024)S(1)} %bitcast.42, ...), kind=kOutput, calls=%fused_computation.17 | convolution fusion | flops 2155872000 | bytes 12625408 | tf_op jit(solution)/shard_map/dot_general | solution.py:163
  19.3 0.6 multiply_reduce_fusion.1
  20.2 2.1 %convolution_convert_fusion.1 = bf16[384,2048]{1,0:T(8,128)(2,1)} fusion(pred[256,384]{1,0:T(32,128)(4,1)S(1)} %get-tuple-element.6, bf16[256,2048]{1,0:T(8,128)(2,1)S(1)} %get-tuple-element.22, bf16[256,2048]{1,0:T(8,128)(2,1)S(1)} %copy-done.3, f32[2048]{0:T(1024)S(1)} %bitcast.39, f32[256]{0:T(256)S(1)} %add_rsqrt_fusion.1, f32[2048]{0:T(1024)S(1)} %bitcast.35, ...), kind=kOutput, calls=%fused_computation.1 | convolution fusion | flops 407633920 | bytes 3786752 | tf_op jit(solution)/shard_map/dot_general | solution.py:30
  22.3 5.0 %all-to-all-start = ((bf16[16,24,2048]{2,1,0:T(8,128)(2,1)}), bf16[16,24,2048]{2,1,0:T(8,128)(2,1)S(1)}, u32[]{:S(2)}, u32[]{:S(2)}) async-start(bf16[16,24,2048]{2,1,0:T(8,128)(2,1)} %bitcast.33), calls=%async_computation | async-start | bytes 3145728 | tf_op jit(solution)/shard_map/all_to_all | solution.py:175
  27.3 3.3 %convolution_convert_fusion = bf16[384,2048]{1,0:T(8,128)(2,1)} fusion(pred[256,384]{1,0:T(32,128)(4,1)S(1)} %get-tuple-element.5, bf16[256,2048]{1,0:T(8,128)(2,1)} %copy-done.5, bf16[256,2048]{1,0:T(8,128)(2,1)S(1)} %copy-done.3, f32[2048]{0:T(1024)S(1)} %bitcast.40, f32[256]{0:T(256)S(1)} %add_rsqrt_fusion.1, f32[2048]{0:T(1024)S(1)} %bitcast.36, ...), kind=kOutput, calls=%fused_computation | convolution fusion | flops 407633920 | bytes 3786752 | tf_op jit(solution)/shard_map/dot_general | solution.py:30
  30.6 32.9 %all-to-all-done = bf16[16,24,2048]{2,1,0:T(8,128)(2,1)S(1)} async-done(((bf16[16,24,2048]{2,1,0:T(8,128)(2,1)}), bf16[16,24,2048]{2,1,0:T(8,128)(2,1)S(1)}, u32[]{:S(2)}, u32[]{:S(2)}) %all-to-all-start) | async-done | bytes 1572896 | tf_op jit(solution)/shard_map/all_to_all | solution.py:175
  63.5 4.8 %all-to-all-start.2 = ((bf16[16,24,2048]{2,1,0:T(8,128)(2,1)}), bf16[16,24,2048]{2,1,0:T(8,128)(2,1)S(1)}, u32[]{:S(2)}, u32[]{:S(2)}) async-start(bf16[16,24,2048]{2,1,0:T(8,128)(2,1)} %bitcast.32), calls=%async_computation.2 | async-start | bytes 3145728 | tf_op jit(solution)/shard_map/all_to_all | solution.py:175
  68.3 26.9 %experts.2 = bf16[384,2048]{1,0:T(8,128)(2,1)S(1)} custom-call(bf16[384,2048]{1,0:T(8,128)(2,1)S(1)} %bitcast.25, bf16[1,2048,4096]{2,1,0:T(8,128)(2,1)} %gate_ref.3, bf16[1,2048,4096]{2,1,0:T(8,128)(2,1)} %up_ref.3, bf16[1,4096,2048]{2,1,0:T(8,128)(2,1)} %down_ref.3), custom_call_target="tpu_custom_call" | custom-call | flops 19327352832 | bytes 53477376 | tf_op jit(solution)/shard_map/experts/pallas_call | solution.py:91
  95.2 1.2 copy-done
  96.4 8.1 %all-to-all-done.2 = bf16[16,24,2048]{2,1,0:T(8,128)(2,1)S(1)} async-done(((bf16[16,24,2048]{2,1,0:T(8,128)(2,1)}), bf16[16,24,2048]{2,1,0:T(8,128)(2,1)S(1)}, u32[]{:S(2)}, u32[]{:S(2)}) %all-to-all-start.2) | async-done | bytes 1572896 | tf_op jit(solution)/shard_map/all_to_all | solution.py:175
  104.4 4.8 %all-to-all-start.1 = ((bf16[16,24,2048]{2,1,0:T(8,128)(2,1)}), bf16[16,24,2048]{2,1,0:T(8,128)(2,1)S(1)}, u32[]{:S(2)}, u32[]{:S(2)}) async-start(bf16[16,24,2048]{2,1,0:T(8,128)(2,1)} %bitcast.27), calls=%async_computation.1 | async-start | bytes 3145728 | tf_op jit(solution)/shard_map/all_to_all | solution.py:179
  109.2 28.1 %experts.3 = bf16[384,2048]{1,0:T(8,128)(2,1)} custom-call(bf16[384,2048]{1,0:T(8,128)(2,1)S(1)} %bitcast.26, bf16[1,2048,4096]{2,1,0:T(8,128)(2,1)} %gate_ref.3, bf16[1,2048,4096]{2,1,0:T(8,128)(2,1)} %up_ref.3, bf16[1,4096,2048]{2,1,0:T(8,128)(2,1)} %down_ref.3), custom_call_target="tpu_custom_call" | custom-call | flops 19327352832 | bytes 53477376 | tf_op jit(solution)/shard_map/experts/pallas_call | solution.py:91
  137.3 8.1 %all-to-all-done.1 = bf16[16,24,2048]{2,1,0:T(8,128)(2,1)S(1)} async-done(((bf16[16,24,2048]{2,1,0:T(8,128)(2,1)}), bf16[16,24,2048]{2,1,0:T(8,128)(2,1)S(1)}, u32[]{:S(2)}, u32[]{:S(2)}) %all-to-all-start.1) | async-done | bytes 1572896 | tf_op jit(solution)/shard_map/all_to_all | solution.py:179
  145.4 1.2 copy-done.1
  146.6 5.0 %all-to-all-start.3 = ((bf16[16,24,2048]{2,1,0:T(8,128)(2,1)}), bf16[16,24,2048]{2,1,0:T(8,128)(2,1)S(1)}, u32[]{:S(2)}, u32[]{:S(2)}) async-start(bf16[16,24,2048]{2,1,0:T(8,128)(2,1)} %bitcast.15), calls=%async_computation.3 | async-start | bytes 3145728 | tf_op jit(solution)/shard_map/all_to_all | solution.py:179
  151.6 0.3 fusion.32
  151.9 0.3 fusion.30
  152.3 2.2 %fusion.21 = f32[256,2048]{1,0:T(8,128)S(1)} fusion(bf16[384,2048]{1,0:T(8,128)(2,1)} %bitcast.30, pred[256,384]{1,0:T(32,128)(4,1)S(1)} %get-tuple-element.6, bf16[256,384]{1,0:T(8,128)(2,1)S(1)} %fusion.32), kind=kOutput, calls=%fused_computation.42 | convolution fusion | flops 402751488 | bytes 3964928 | tf_op jit(solution)/shard_map/dot_general | solution.py:30
  154.5 2.1 %convolution_add_fusion.2 = f32[256,2048]{1,0:T(8,128)} fusion(f32[256,2048]{1,0:T(8,128)S(1)} %fusion.21, bf16[384,2048]{1,0:T(8,128)(2,1)S(1)} %bitcast.31, pred[256,384]{1,0:T(32,128)(4,1)S(1)} %get-tuple-element.6, bf16[256,384]{1,0:T(8,128)(2,1)S(1)} %fusion.30), kind=kOutput, calls=%fused_computation.4 | convolution fusion | flops 403275776 | bytes 6062080 | tf_op jit(solution)/shard_map/dot_general | solution.py:30
  156.6 31.1 %all-to-all-done.3 = bf16[16,24,2048]{2,1,0:T(8,128)(2,1)S(1)} async-done(((bf16[16,24,2048]{2,1,0:T(8,128)(2,1)}), bf16[16,24,2048]{2,1,0:T(8,128)(2,1)S(1)}, u32[]{:S(2)}, u32[]{:S(2)}) %all-to-all-start.3) | async-done | bytes 1572896 | tf_op jit(solution)/shard_map/all_to_all | solution.py:179
  187.7 2.3 %convolution_add_fusion.1 = f32[256,2048]{1,0:T(8,128)S(1)} fusion(f32[256,2048]{1,0:T(8,128)} %convolution_add_fusion.2, bf16[384,2048]{1,0:T(8,128)(2,1)S(1)} %bitcast.28, pred[256,384]{1,0:T(32,128)(4,1)S(1)} %get-tuple-element.5, bf16[256,384]{1,0:T(8,128)(2,1)S(1)} %fusion.32), kind=kOutput, calls=%fused_computation.3 | convolution fusion | flops 403275776 | bytes 6062080 | tf_op jit(solution)/shard_map/dot_general | solution.py:30
  190.1 0.8 multiply_reduce_fusion
  190.9 0.3 copy-done.4
  191.3 0.3 copy-done.6
  191.6 1.7 add_convert_fusion
  (42 shorter events, 1.0 us)
Async XLA Ops:
  2.5 7.7 %collective-permute-start = (bf16[2,4224]{1,0:T(2,128)(2,1)S(1)}, bf16[2,4224]{1,0:T(2,128)(2,1)S(1)}, u32[]{:S(2)}, u32[]{:S(2)}) collective-permute-start(bf16[2,4224]{1,0:T(2,128)(2,1)S(1)} %pad_maximum_fusion.1), channel_id=1, source_target_pairs={{0,1},{1,2},{2,3},{3,4},{4,5},{5,6},{6,7},{7,8},{8,9},{9,10},{10,1... | collective-permute-start | bytes 50696 | tf_op jit(solution)/shard_map/ppermute | solution.py:21
  6.3 3.3 %copy-start.11 = (s32[256,2]{0,1:T(2,128)S(1)}, s32[256,2]{0,1:T(2,128)}, u32[]{:S(2)}) copy-start(s32[256,2]{0,1:T(2,128)} %param.21) | copy-start | bytes 6148
  6.3 3.3 %copy-start.7 = (bf16[3,2048]{1,0:T(4,128)(2,1)S(1)}, bf16[3,2048]{1,0:T(4,128)(2,1)}, u32[]{:S(2)}) copy-start(bf16[3,2048]{1,0:T(4,128)(2,1)} %param.17) | copy-start | bytes 36868
  6.3 3.3 %copy-start.8 = (f32[3,2048]{1,0:T(4,128)S(1)}, f32[3,2048]{1,0:T(4,128)}, u32[]{:S(2)}) copy-start(f32[3,2048]{1,0:T(4,128)} %param.20) | copy-start | bytes 73732
  9.6 0.8 copy-start.10
  9.6 1.2 copy-start.12
  10.8 8.4 %copy-start.3 = (bf16[256,2048]{1,0:T(8,128)(2,1)S(1)}, bf16[256,2048]{1,0:T(8,128)(2,1)}, u32[]{:S(2)}) copy-start(bf16[256,2048]{1,0:T(8,128)(2,1)} %param.13) | copy-start | bytes 3145732
  19.2 1.0 copy-start.5
  22.3 41.2 %all-to-all-start = ((bf16[16,24,2048]{2,1,0:T(8,128)(2,1)}), bf16[16,24,2048]{2,1,0:T(8,128)(2,1)S(1)}, u32[]{:S(2)}, u32[]{:S(2)}) async-start(bf16[16,24,2048]{2,1,0:T(8,128)(2,1)} %bitcast.33), calls=%async_computation | async-start | bytes 3145728 | tf_op jit(solution)/shard_map/all_to_all | solution.py:175
  63.5 41.0 %all-to-all-start.2 = ((bf16[16,24,2048]{2,1,0:T(8,128)(2,1)}), bf16[16,24,2048]{2,1,0:T(8,128)(2,1)S(1)}, u32[]{:S(2)}, u32[]{:S(2)}) async-start(bf16[16,24,2048]{2,1,0:T(8,128)(2,1)} %bitcast.32), calls=%async_computation.2 | async-start | bytes 3145728 | tf_op jit(solution)/shard_map/all_to_all | solution.py:175
  95.2 1.2 copy-start
  104.4 41.0 %all-to-all-start.1 = ((bf16[16,24,2048]{2,1,0:T(8,128)(2,1)}), bf16[16,24,2048]{2,1,0:T(8,128)(2,1)S(1)}, u32[]{:S(2)}, u32[]{:S(2)}) async-start(bf16[16,24,2048]{2,1,0:T(8,128)(2,1)} %bitcast.27), calls=%async_computation.1 | async-start | bytes 3145728 | tf_op jit(solution)/shard_map/all_to_all | solution.py:179
  137.3 14.3 %copy-start.9 = (f32[256,2]{0,1:T(2,128)S(1)}, f32[256,2]{0,1:T(2,128)}, u32[]{:S(2)}) copy-start(f32[256,2]{0,1:T(2,128)} %param.22) | copy-start | bytes 6148
  145.4 1.2 copy-start.1
  146.6 41.1 %all-to-all-start.3 = ((bf16[16,24,2048]{2,1,0:T(8,128)(2,1)}), bf16[16,24,2048]{2,1,0:T(8,128)(2,1)S(1)}, u32[]{:S(2)}, u32[]{:S(2)}) async-start(bf16[16,24,2048]{2,1,0:T(8,128)(2,1)} %bitcast.15), calls=%async_computation.3 | async-start | bytes 3145728 | tf_op jit(solution)/shard_map/all_to_all | solution.py:179
  151.9 2.6 %copy-start.2 = (bf16[16,24,2048]{2,1,0:T(8,128)(2,1)S(1)}, bf16[16,24,2048]{2,1,0:T(8,128)(2,1)}, u32[]{:S(2)}) copy-start(bf16[16,24,2048]{2,1,0:T(8,128)(2,1)} %copy-done.1) | copy-start | bytes 4718596
  190.0 1.2 copy-start.4
  190.0 1.5 copy-start.6

commit v2 on v1

--- a/solution.py
+++ b/solution.py
@@ -1,3 +1,4 @@
+import functools
 import math
 
 import jax
@@ -63,8 +64,118 @@
     return onehot, w_high, w_low
 
 
-def expert_body(rows_ref, gate_ref, up_ref, down_ref, out_ref, acc_ref):
+def expert_block(rows, w_gate, w_up, w_down):
+    return expert_blocks([rows], w_gate, w_up, w_down)[0]
+
+
+def earlier_than(rows, axis):
+    i = lax.broadcasted_iota(jnp.int32, (rows, rows), axis)
+    j = lax.broadcasted_iota(jnp.int32, (rows, rows), 1 - axis)
+    return jnp.where(i < j, 1.0, 0.0).astype(jnp.bfloat16)
+
+
+def pick_body(partners, cap, routes_ref, normed_ref, *out_refs):
+    rows = normed_ref.shape[0]
+    ids = lax.broadcasted_iota(jnp.int32, (partners, rows), 0)
+    named = jnp.zeros((partners, rows), jnp.float32)
+    for k in range(TOP):
+        named = named + jnp.where(routes_ref[k : k + 1, :] == ids, 1.0, 0.0)
+    before = dot_f32(named.astype(jnp.bfloat16), earlier_than(rows, 0), ((1,), (0,)))
+    slot_of = jnp.where(named > 0.0, before, -1.0).astype(jnp.bfloat16)
+    group = math.gcd(partners, 4)
+    normed = normed_ref[...]
+    for first in range(0, partners, group):
+        line = lax.broadcasted_iota(jnp.int32, (group * cap, partners), 0)
+        start = (lax.broadcasted_iota(jnp.int32, (group * cap, partners), 1) - first) * cap
+        mine = (line >= start) & (line < start + cap)
+        slot = jnp.sum(jnp.where(mine, (line - start).astype(jnp.float32), 0.0), axis=1, keepdims=True)
+        spread = jnp.where(mine, 1.0, 0.0).astype(jnp.bfloat16)
+        taken = dot_f32(spread, slot_of, ((1,), (0,))) == slot
+        onehot = jnp.where(taken, 1.0, 0.0).astype(jnp.bfloat16)
+        picked = dot_f32(onehot, normed, ((1,), (0,))).astype(jnp.bfloat16)
+        for b in range(group):
+            out_refs[first + b][...] = picked[b * cap : (b + 1) * cap]
+
+
+def pick_blocks(partner_t, normed, partners, cap):
+    width = normed.shape[1]
+    return pl.pallas_call(
+        functools.partial(pick_body, partners, cap),
+        out_shape=[jax.ShapeDtypeStruct((cap, width), jnp.bfloat16)] * partners,
+        compiler_params=pltpu.CompilerParams(vmem_limit_bytes=48 * 2**20),
+        name="pick",
+    )(partner_t, normed)
+
+
+def share_columns(partner, share, partners, first, count, cap):
+    rows = partner.shape[0]
+    ids = lax.broadcasted_iota(jnp.int32, (rows, partners), 1)
+    total = share[:, 0:1]
+    for k in range(1, TOP):
+        total = total + share[:, k : k + 1]
+    named = jnp.zeros((rows, partners), jnp.float32)
+    share_of = jnp.zeros((rows, partners), jnp.float32)
+    for k in range(TOP):
+        hit = partner[:, k : k + 1] == ids
+        named = named + jnp.where(hit, 1.0, 0.0)
+        share_of = share_of + jnp.where(hit, share[:, k : k + 1] / total, 0.0)
+    before = dot_f32(earlier_than(rows, 1), named.astype(jnp.bfloat16), ((1,), (0,)))
+    slot_of = jnp.where(named > 0.0, before, -1.0).astype(jnp.bfloat16)
+    high = share_of.astype(jnp.bfloat16)
+    low = (share_of - high.astype(jnp.float32)).astype(jnp.bfloat16)
+    cols = lax.broadcasted_iota(jnp.int32, (partners, count * cap), 1)
+    start = (lax.broadcasted_iota(jnp.int32, (partners, count * cap), 0) - first) * cap
+    mine = (cols >= start) & (cols < start + cap)
+    slot = jnp.sum(jnp.where(mine, (cols - start).astype(jnp.float32), 0.0), axis=0, keepdims=True)
+    spread = jnp.where(mine, 1.0, 0.0).astype(jnp.bfloat16)
+    taken = dot_f32(slot_of, spread, ((1,), (0,))) == slot
+    return [
+        jnp.where(taken, dot_f32(part, spread, ((1,), (0,))), 0.0).astype(jnp.bfloat16) for part in (high, low)
+    ]
+
+
+def weighted_sum(partners, first, partner_ref, share_ref, block_refs, rows_ref):
+    cap = block_refs[0].shape[0]
+    for b, ref in enumerate(block_refs):
+        rows_ref[b * cap : (b + 1) * cap, :] = ref[...]
+    high, low = share_columns(partner_ref[...], share_ref[...], partners, first, len(block_refs), cap)
+    rows = rows_ref[...]
+    return dot_f32(high, rows, ((1,), (0,))) + dot_f32(low, rows, ((1,), (0,)))
+
+
+def join_body(partners, first, partner_ref, share_ref, *refs):
+    *block_refs, out_ref, rows_ref = refs
+    out_ref[...] = weighted_sum(partners, first, partner_ref, share_ref, block_refs, rows_ref)
+
+
+def last_body(partners, first, partner_ref, share_ref, gain_ref, stream_ref, part_ref, *refs):
+    *block_refs, out_ref, rows_ref = refs
+    combined = part_ref[...] + weighted_sum(partners, first, partner_ref, share_ref, block_refs, rows_ref)
+    out_ref[...] = (stream_ref[...] + rms_scale(combined, gain_ref[...])).astype(out_ref.dtype)
+
+
+def join_call(body, partners, first, given, blocks, out):
+    cap, width = blocks[0].shape
+    return pl.pallas_call(
+        functools.partial(body, partners, first),
+        out_shape=out,
+        scratch_shapes=[pltpu.VMEM((len(blocks) * cap, width), jnp.bfloat16)],
+        compiler_params=pltpu.CompilerParams(vmem_limit_bytes=48 * 2**20),
+        name="join",
+    )(*given, *blocks)
+
+
+def expert_body(count, *refs):
+    in_refs, (gate_ref, up_ref, down_ref) = refs[:count], refs[count : count + 3]
+    out_refs, (rows_ref, acc_ref) = refs[count + 3 : -2], refs[-2:]
     step = pl.program_id(0)
+    cap = in_refs[0].shape[0]
+
+    @pl.when(step == 0)
+    def _():
+        for b, ref in enumerate(in_refs):
+            rows_ref[b * cap : (b + 1) * cap, :] = ref[...]
+
     rows = rows_ref[...]
     gate_proj = jnp.dot(rows, gate_ref[0], preferred_element_type=jnp.float32)
     up_proj = jnp.dot(rows, up_ref[0], preferred_element_type=jnp.float32)
@@ -81,25 +192,28 @@
 
     @pl.when(step == pl.num_programs(0) - 1)
     def _():
-        out_ref[...] = acc_ref[...].astype(out_ref.dtype)
-
-
-def expert_block(rows, w_gate, w_up, w_down):
-    count, width = rows.shape
+        for b, ref in enumerate(out_refs):
+            ref[...] = acc_ref[b * cap : (b + 1) * cap, :].astype(ref.dtype)
+
+
+def expert_blocks(blocks, w_gate, w_up, w_down):
+    cap, width = blocks[0].shape
     units = w_gate.shape[2]
     block = math.gcd(units, 512)
+    count = len(blocks) * cap
+    whole = pl.BlockSpec((cap, width), lambda j: (0, 0))
     return pl.pallas_call(
-        expert_body,
+        functools.partial(expert_body, len(blocks)),
         grid=(units // block,),
         in_specs=[
-            pl.BlockSpec((count, width), lambda j: (0, 0)),
+            *[whole] * len(blocks),
             pl.BlockSpec((1, width, block), lambda j: (0, 0, j)),
             pl.BlockSpec((1, width, block), lambda j: (0, 0, j)),
             pl.BlockSpec((1, block, width), lambda j: (0, j, 0)),
         ],
-        out_specs=pl.BlockSpec((count, width), lambda j: (0, 0)),
-        out_shape=jax.ShapeDtypeStruct((count, width), jnp.bfloat16),
-        scratch_shapes=[pltpu.VMEM((count, width), jnp.float32)],
+        out_specs=[whole] * len(blocks),
+        out_shape=[jax.ShapeDtypeStruct((cap, width), jnp.bfloat16)] * len(blocks),
+        scratch_shapes=[pltpu.VMEM((count, width), jnp.bfloat16), pltpu.VMEM((count, width), jnp.float32)],
         cost_estimate=pl.CostEstimate(
             flops=6 * count * width * units,
             transcendentals=count * units,
@@ -109,7 +223,49 @@
             dimension_semantics=("arbitrary",), vmem_limit_bytes=48 * 2**20
         ),
         name="experts",
-    )(rows, w_gate, w_up, w_down)
+    )(*blocks, w_gate, w_up, w_down)
+
+
+def by_partner(partners):
+    half, quarter = partners // 2, partners // 4
+    return [range(half, half + quarter), range(half), range(half + quarter, partners)]
+
+
+def crossed(block, partner):
+    return lax.ppermute(block, "sp", [(i, i ^ partner) for i in range(lax.axis_size("sp"))])
+
+
+def routed_experts(stream, normed, routes, route_weights, gain, w_gate, w_up, w_down, cap):
+    partners = lax.axis_size("sp")
+    partner = routes ^ lax.axis_index("sp")
+    blocks = list(pick_blocks(partner.T, normed, partners, cap))
+    groups = by_partner(partners)
+    for b in [*groups[0], *groups[2], *groups[1]]:
+        if b > 0:
+            blocks[b] = crossed(blocks[b], b)
+    results = {}
+    for group in groups:
+        worked = expert_blocks([blocks[b] for b in group], w_gate, w_up, w_down)
+        for b, block in zip(group, worked):
+            results[b] = crossed(block, b) if b > 0 else block
+    rows, width = stream.shape
+    early = groups[2][0]
+    part = join_call(
+        join_body,
+        partners,
+        0,
+        (partner, route_weights),
+        [results[b] for b in range(early)],
+        jax.ShapeDtypeStruct((rows, width), jnp.float32),
+    )
+    return join_call(
+        last_body,
+        partners,
+        early,
+        (partner, route_weights, gain, stream, part),
+        [results[b] for b in groups[2]],
+        jax.ShapeDtypeStruct((rows, width), jnp.bfloat16),
+    )
 
 
 def mixer_rows(gate_b, gate_c, value, taps, doc_ids):
@@ -130,6 +286,10 @@
         same_doc = ext_ids[tap_reach - distance : tap_reach - distance + tok_dev] == id_values
         convolved = convolved + jnp.where(same_doc[:, None], tap_weights[distance] * earlier, 0.0)
     return (gate_b.astype(jnp.float32) * convolved).astype(jnp.bfloat16)
+
+
+def by_partners(lanes, experts):
+    return lanes == 1 and experts >= 4 and experts & (experts - 1) == 0
 
 
 def per_device(
@@ -154,9 +314,6 @@
     offset = lax.axis_index("tp") * rows_blk
     my_routes = lax.dynamic_slice_in_dim(routes, offset, rows_blk, 0)
     my_weights = lax.dynamic_slice_in_dim(route_weights, offset, rows_blk, 0)
-    tables = route_tables(my_routes, my_weights, experts)
-    edges = [capacity * c // CHUNKS for c in range(CHUNKS + 1)]
-    chunks = [chunk_tables(tables, experts, a, b - a) for a, b in zip(edges, edges[1:])]
 
     mixed = mixer_rows(gate_b, gate_c, value, taps, doc_ids)
     projected = lax.psum_scatter(
@@ -168,6 +325,14 @@
     stream = resid.astype(jnp.float32) + rms_scale(projected, norm_gains[0])
     normed = rms_scale(stream, norm_gains[1]).astype(jnp.bfloat16)
 
+    if by_partners(lax.axis_size("tp"), experts):
+        return routed_experts(
+            stream, normed, my_routes, my_weights, norm_gains[2:3], w_gate, w_up, w_down, capacity
+        )
+
+    tables = route_tables(my_routes, my_weights, experts)
+    edges = [capacity * c // CHUNKS for c in range(CHUNKS + 1)]
+    chunks = [chunk_tables(tables, experts, a, b - a) for a, b in zip(edges, edges[1:])]
     combined = 0.0
     for (onehot, w_high, w_low), first, last in zip(chunks, edges, edges[1:]):
         size = last - first

time: 194 us -> 213 us (1.098)
  starting transfers between devices: 23.2 us -> 58.2 us
  waiting for transfers between devices: 80.2 us -> 54.3 us
  Pallas kernels: 55 us -> 76 us
  matrix products: 22.4 us -> 6.53 us
  local copies, waits for them, and re-layouts: 5.56 us -> 13.2 us
  other arithmetic: 6.61 us -> 3.85 us
    all_to_all x4 -> x0, waiting for transfers between devices: 80.2 us -> none  [the longest x2 41 us: per_device(): lax.all_to_all(outgoing.reshape(experts, size, width), 'sp', split_axis=0...]
    ppermute x0 -> x30, starting transfers between devices: none -> 54.5 us  [crossed(): lax.ppermute(block, 'sp', [(i, i ^ partner) for i in range(lax.axis_size(...]
    ppermute x0 -> x30, waiting for transfers between devices: none -> 54.3 us  [crossed(): lax.ppermute(block, 'sp', [(i, i ^ partner) for i in range(lax.axis_size(...]
    pallas_call x2 -> x6, Pallas kernels: 55 us -> 76 us  [the longest x3 68.9 us: expert_blocks(): pl.pallas_call(functools.partial(expert_body, len(blocks)), grid=(units /...]
    all_to_all x4 -> x0, starting transfers between devices: 19.5 us -> none  [the longest x2 9.76 us: per_device(): lax.all_to_all(outgoing.reshape(experts, size, width), 'sp', split_axis=0...]
    dot_general x9 -> x0, matrix products: 14 us -> none  [dot_f32(): lax.dot_general(a, b, (dims, ((), ())), preferred_element_type=jnp.float32)]
    unnamed x26 -> x44, local copies, waits for them, and re-layouts: 3.7 us -> 11.3 us
  transfers between devices with their start and end apart: 5 -> 31, of which waited for: 4 -> 11; matrix products, arithmetic and copies ran while one was open for 6% -> 1% of each run, Pallas kernels for 28% -> 34%
where the time goes in v2:
time: 213 us; the launch traced here: 212 us
  Pallas kernels  76 us (36%)
  starting transfers between devices  58.2 us (27%)
  waiting for transfers between devices  54.3 us (25%)
  local copies, waits for them, and re-layouts  13.2 us (6%)
  matrix products  6.53 us (3%)
  other arithmetic  3.85 us (2%)
    pallas_call x3, Pallas kernels, expert_blocks(): pl.pallas_call(functools.partial(expert_body, len(blocks)), grid=(units /...  68.9 us
    ppermute x30, starting transfers between devices, crossed(): lax.ppermute(block, 'sp', [(i, i ^ partner) for i in range(lax.axis_size(...  54.5 us
    ppermute x30, waiting for transfers between devices, crossed(): lax.ppermute(block, 'sp', [(i, i ^ partner) for i in range(lax.axis_size(...  54.3 us
    unnamed x44, local copies, waits for them, and re-layouts  11.3 us
    dot_general x1, matrix products, per_device(): jnp.dot(mixed, out_weight, preferred_element_type=jnp.float32)  6.53 us
    pallas_call x2, Pallas kernels, join_call(): pl.pallas_call(functools.partial(body, partners, first), out_shape=out, s...  4.93 us
  transfers between devices with their start and end apart: 31, of which 11 were waited for; matrix products, arithmetic and copies ran while one was open for 1% of the time, Pallas kernels for 34%

profile of v2, /device:TPU:11, one launch (start us, length us, event | category | flops | bytes accessed | tf_op | source)
XLA Modules:
  0.0 212.4 jit_solution(5151780399629900142)
XLA Ops:
  2.5 3.7 %collective-permute-start = (bf16[2,4224]{1,0:T(2,128)(2,1)S(1)}, bf16[2,4224]{1,0:T(2,128)(2,1)S(1)}, u32[]{:S(2)}, u32[]{:S(2)}) collective-permute-start(bf16[2,4224]{1,0:T(2,128)(2,1)S(1)} %pad_maximum_fusion.1), channel_id=1, source_target_pairs={{0,1},{1,2},{2,3},{3,4},{4,5},{5,6},{6,7},{7,8},{8,9},{9,10},{10,1... | collective-permute-start | bytes 50696 | tf_op jit(solution)/shard_map/ppermute | solution.py:22
  6.3 2.0 convert_multiply_fusion.2
  8.9 6.5 %fusion.7 = (f32[256]{0:T(256)S(1)}, bf16[256,2048]{1,0:T(8,128)(2,1)S(1)}) fusion(bf16[2048,2048]{1,0:T(8,128)(2,1)} %param.19, f32[2,2048]{1,0:T(2,128)S(1)} %slice_multiply_fusion, f32[256,2048]{1,0:T(8,128)S(1)} %convert_multiply_fusion.2, bf16[256,2048]{1,0:T(8,128)(2,1)S(1)} %copy-done.20, f32[2048]{0:T(1024)S(1)} %bitcast.12, f32[2048]{0:T(1024)S(1)} %bitcast.11, ...), kind=kOutput, calls=%fused_computation.12 | convolution fusion | flops 2155872000 | bytes 12625408 | tf_op jit(solution)/shard_map/dot_general | solution.py:320
  16.4 2.1 pick.1
  21.2 1.4 collective-permute-start.3
  22.8 1.2 collective-permute-start.5
  25.0 1.5 collective-permute-done.2.refs_2_
  27.2 2.3 %collective-permute-start.7 = (bf16[48,2048]{1,0:T(8,128)(2,1)}, bf16[48,2048]{1,0:T(8,128)(2,1)}, u32[]{:S(2)}, u32[]{:S(2)}) collective-permute-start(bf16[48,2048]{1,0:T(8,128)(2,1)} %get-tuple-element.44), channel_id=1, source_target_pairs={{0,7},{1,6},{2,5},{3,4},{4,3},{5,2},{6,1},{7,0},{8,15},{9,14},{10,... | collective-permute-start | bytes 589832 | tf_op jit(solution)/shard_map/ppermute | solution.py:235
  29.5 2.2 %collective-permute-done.3.refs_3_ = bf16[48,2048]{1,0:T(8,128)(2,1)S(1)} collective-permute-done((bf16[48,2048]{1,0:T(8,128)(2,1)S(1)}, bf16[48,2048]{1,0:T(8,128)(2,1)S(1)}, u32[]{:S(2)}, u32[]{:S(2)}) %collective-permute-start.3) | collective-permute-done | bytes 196640 | tf_op jit(solution)/shard_map/ppermute | solution.py:235
  32.3 1.9 collective-permute-start.15
  35.7 3.3 %collective-permute-start.17 = (bf16[48,2048]{1,0:T(8,128)(2,1)}, bf16[48,2048]{1,0:T(8,128)(2,1)S(1)}, u32[]{:S(2)}, u32[]{:S(2)}) collective-permute-start(bf16[48,2048]{1,0:T(8,128)(2,1)} %get-tuple-element.55), channel_id=1, source_target_pairs={{0,10},{1,11},{2,8},{3,9},{4,14},{5,15},{6,12},{7,13},{8,2},{9,3},... | collective-permute-start | bytes 589832 | tf_op jit(solution)/shard_map/ppermute | solution.py:235
  39.1 5.1 %collective-permute-done.6.refs_6_ = bf16[48,2048]{1,0:T(8,128)(2,1)} collective-permute-done((bf16[48,2048]{1,0:T(8,128)(2,1)}, bf16[48,2048]{1,0:T(8,128)(2,1)}, u32[]{:S(2)}, u32[]{:S(2)}) %collective-permute-start.6) | collective-permute-done | bytes 196640 | tf_op jit(solution)/shard_map/ppermute | solution.py:235
  44.1 3.5 %collective-permute-start.18 = (bf16[48,2048]{1,0:T(8,128)(2,1)}, bf16[48,2048]{1,0:T(8,128)(2,1)S(1)}, u32[]{:S(2)}, u32[]{:S(2)}) collective-permute-start(bf16[48,2048]{1,0:T(8,128)(2,1)} %copy-done.1), channel_id=1, source_target_pairs={{0,11},{1,10},{2,9},{3,8},{4,15},{5,14},{6,13},{7,12},{8,3},{9,2},... | collective-permute-start | bytes 589832 | tf_op jit(solution)/shard_map/ppermute | solution.py:235
  49.1 1.5 collective-permute-start.24
  50.6 17.8 %collective-permute-done.16.refs_1_ = bf16[48,2048]{1,0:T(8,128)(2,1)S(1)} collective-permute-done((bf16[48,2048]{1,0:T(8,128)(2,1)}, bf16[48,2048]{1,0:T(8,128)(2,1)S(1)}, u32[]{:S(2)}, u32[]{:S(2)}) %collective-permute-start.16) | collective-permute-done | bytes 196640 | tf_op jit(solution)/shard_map/ppermute | solution.py:235
  68.4 4.2 %collective-permute-done.17.refs_2_ = bf16[48,2048]{1,0:T(8,128)(2,1)S(1)} collective-permute-done((bf16[48,2048]{1,0:T(8,128)(2,1)}, bf16[48,2048]{1,0:T(8,128)(2,1)S(1)}, u32[]{:S(2)}, u32[]{:S(2)}) %collective-permute-start.17) | collective-permute-done | bytes 196640 | tf_op jit(solution)/shard_map/ppermute | solution.py:235
  78.8 27.7 %experts.3 = (bf16[48,2048]{1,0:T(8,128)(2,1)S(1)}, bf16[48,2048]{1,0:T(8,128)(2,1)S(1)}, bf16[48,2048]{1,0:T(8,128)(2,1)S(1)}, bf16[48,2048]{1,0:T(8,128)(2,1)S...) custom-call(bf16[48,2048]{1,0:T(8,128)(2,1)S(1)} %copy-done.3, ...), custom_call_target="tpu_custom_call" | custom-call | flops 19327352832 | bytes 53477376 | tf_op jit(solution)/shard_map/experts/pallas_call | solution.py:205
  108.9 5.4 %collective-permute-start.11 = (bf16[48,2048]{1,0:T(8,128)(2,1)S(1)}, bf16[48,2048]{1,0:T(8,128)(2,1)S(1)}, u32[]{:S(2)}, u32[]{:S(2)}) collective-permute-start(bf16[48,2048]{1,0:T(8,128)(2,1)S(1)} %get-tuple-element.49), channel_id=1, source_target_pairs={{0,4},{1,5},{2,6},{3,7},{4,0},{5,1},{6,2},{7,3},{8,12},{9,13},{10,... | collective-permute-start | bytes 589832 | tf_op jit(solution)/shard_map/ppermute | solution.py:235
  114.3 20.6 %experts.4 = (bf16[48,2048]{1,0:T(8,128)(2,1)S(1)}, bf16[48,2048]{1,0:T(8,128)(2,1)S(1)}, bf16[48,2048]{1,0:T(8,128)(2,1)S(1)}, bf16[48,2048]{1,0:T(8,128)(2,1)S(1)}) custom-call(bf16[48,2048]{1,0:T(8,128)(2,1)S(1)} %collective-permute-done.15.refs_0_, bf16[48,2048]{1,0:T(8,128)(2,1)S(1)} %collective-permute-done.16.refs_1_, ...), custom_call_target="tpu_custom_call" | custom-call | flops 9663676416 | bytes 51904512 | tf_op jit(solution)/shard_map/experts/pallas_call | solution.py:205
  134.9 2.4 %collective-permute-start.13 = (bf16[48,2048]{1,0:T(8,128)(2,1)S(1)}, bf16[48,2048]{1,0:T(8,128)(2,1)S(1)}, u32[]{:S(2)}, u32[]{:S(2)}) collective-permute-start(bf16[48,2048]{1,0:T(8,128)(2,1)S(1)} %get-tuple-element.51), channel_id=1, source_target_pairs={{0,6},{1,7},{2,4},{3,5},{4,2},{5,3},{6,0},{7,1},{8,14},{9,15},{10,... | collective-permute-start | bytes 589832 | tf_op jit(solution)/shard_map/ppermute | solution.py:235
  138.0 2.6 %collective-permute-start.20 = (bf16[48,2048]{1,0:T(8,128)(2,1)S(1)}, bf16[48,2048]{1,0:T(8,128)(2,1)S(1)}, u32[]{:S(2)}, u32[]{:S(2)}) collective-permute-start(bf16[48,2048]{1,0:T(8,128)(2,1)S(1)} %get-tuple-element.58), channel_id=1, source_target_pairs={{0,9},{1,8},{2,11},{3,10},{4,13},{5,12},{6,15},{7,14},{8,1},{9,0},... | collective-permute-start | bytes 589832 | tf_op jit(solution)/shard_map/ppermute | solution.py:235
  141.3 20.6 %experts.5 = (bf16[48,2048]{1,0:T(8,128)(2,1)S(1)}, bf16[48,2048]{1,0:T(8,128)(2,1)S(1)}, bf16[48,2048]{1,0:T(8,128)(2,1)S(1)}, bf16[48,2048]{1,0:T(8,128)(2,1)S(1)}) custom-call(bf16[48,2048]{1,0:T(8,128)(2,1)S(1)} %collective-permute-done.23.refs_0_, bf16[48,2048]{1,0:T(8,128)(2,1)S(1)} %collective-permute-done.24.refs_1_, ...), custom_call_target="tpu_custom_call" | custom-call | flops 9663676416 | bytes 51904512 | tf_op jit(solution)/shard_map/experts/pallas_call | solution.py:205
  161.9 3.0 %collective-permute-start.22 = (bf16[48,2048]{1,0:T(8,128)(2,1)S(1)}, bf16[48,2048]{1,0:T(8,128)(2,1)S(1)}, u32[]{:S(2)}, u32[]{:S(2)}) collective-permute-start(bf16[48,2048]{1,0:T(8,128)(2,1)S(1)} %get-tuple-element.60), channel_id=1, source_target_pairs={{0,11},{1,10},{2,9},{3,8},{4,15},{5,14},{6,13},{7,12},{8,3},{9,2},... | collective-permute-start | bytes 589832 | tf_op jit(solution)/shard_map/ppermute | solution.py:235
  165.1 1.4 collective-permute-start.28
  167.5 17.2 %collective-permute-start.30 = (bf16[48,2048]{1,0:T(8,128)(2,1)S(1)}, bf16[48,2048]{1,0:T(8,128)(2,1)S(1)}, u32[]{:S(2)}, u32[]{:S(2)}) collective-permute-start(bf16[48,2048]{1,0:T(8,128)(2,1)S(1)} %get-tuple-element.68), channel_id=1, source_target_pairs={{0,15},{1,14},{2,13},{3,12},{4,11},{5,10},{6,9},{7,8},{8,7},{9,6},... | collective-permute-start | bytes 589832 | tf_op jit(solution)/shard_map/ppermute | solution.py:235
  184.6 1.5 collective-permute-done.22.refs_11_
  186.1 2.4 %join.2.part_ref = f32[256,2048]{1,0:T(8,128)S(1)} custom-call(s32[256,2]{1,0:T(8,128)S(1)} %broadcast_xor_fusion.partner_ref, f32[256,2]{1,0:T(8,128)S(1)} %copy.17.share_ref, bf16[48,2048]{1,0:T(8,128)(2,1)S(1)} %get-tuple-element.45.refs_0_, bf16[48,2048]{1,0:T(8,128)(2,1)S(1)} %collective-permute-done.8.refs_1_, ...), custom_call_target="tpu_custom_call" | custom-call | tf_op jit(solution)/shard_map/join/pallas_call | solution.py:159
  188.5 7.7 %collective-permute-done.27.refs_0_ = bf16[48,2048]{1,0:T(8,128)(2,1)S(1)} collective-permute-done((bf16[48,2048]{1,0:T(8,128)(2,1)S(1)}, bf16[48,2048]{1,0:T(8,128)(2,1)S(1)}, u32[]{:S(2)}, u32[]{:S(2)}) %collective-permute-start.27) | collective-permute-done | bytes 196640 | tf_op jit(solution)/shard_map/ppermute | solution.py:235
  196.3 4.5 %collective-permute-done.28.refs_1_ = bf16[48,2048]{1,0:T(8,128)(2,1)S(1)} collective-permute-done((bf16[48,2048]{1,0:T(8,128)(2,1)S(1)}, bf16[48,2048]{1,0:T(8,128)(2,1)S(1)}, u32[]{:S(2)}, u32[]{:S(2)}) %collective-permute-start.28) | collective-permute-done | bytes 196640 | tf_op jit(solution)/shard_map/ppermute | solution.py:235
  200.8 4.8 %collective-permute-done.29.refs_2_ = bf16[48,2048]{1,0:T(8,128)(2,1)S(1)} collective-permute-done((bf16[48,2048]{1,0:T(8,128)(2,1)S(1)}, bf16[48,2048]{1,0:T(8,128)(2,1)S(1)}, u32[]{:S(2)}, u32[]{:S(2)}) %collective-permute-start.29) | collective-permute-done | bytes 196640 | tf_op jit(solution)/shard_map/ppermute | solution.py:235
  205.6 4.2 %collective-permute-done.30.refs_3_ = bf16[48,2048]{1,0:T(8,128)(2,1)S(1)} collective-permute-done((bf16[48,2048]{1,0:T(8,128)(2,1)S(1)}, bf16[48,2048]{1,0:T(8,128)(2,1)S(1)}, u32[]{:S(2)}, u32[]{:S(2)}) %collective-permute-start.30) | collective-permute-done | bytes 196640 | tf_op jit(solution)/shard_map/ppermute | solution.py:235
  209.8 2.5 %join.3 = bf16[256,2048]{1,0:T(8,128)(2,1)} custom-call(s32[256,2]{1,0:T(8,128)S(1)} %broadcast_xor_fusion.partner_ref, f32[256,2]{1,0:T(8,128)S(1)} %copy.17.share_ref, f32[1,2048]{1,0:T(1,128)S(1)} %get-tuple-element.72.gain_ref, f32[256,2048]{1,0:T(8,128)S(1)} %get-tuple-element.70.stream_ref, f32[256,2048]{1,0:T(8,128)S(1)} %join.2.part_ref, ...), custom_call_target="tpu_custom_call" | custom-call | tf_op jit(solution)/shard_map/join/pallas_call | solution.py:159
  (102 shorter events, 23.3 us)
Async XLA Ops:
  2.5 6.1 %collective-permute-start = (bf16[2,4224]{1,0:T(2,128)(2,1)S(1)}, bf16[2,4224]{1,0:T(2,128)(2,1)S(1)}, u32[]{:S(2)}, u32[]{:S(2)}) collective-permute-start(bf16[2,4224]{1,0:T(2,128)(2,1)S(1)} %pad_maximum_fusion.1), channel_id=1, source_target_pairs={{0,1},{1,2},{2,3},{3,4},{4,5},{5,6},{6,7},{7,8},{8,9},{9,10},{10,1... | collective-permute-start | bytes 50696 | tf_op jit(solution)/shard_map/ppermute | solution.py:22
  16.1 22.8 %copy-start.19 = (f32[256,2]{0,1:T(2,128)S(1)}, f32[256,2]{0,1:T(2,128)}, u32[]{:S(2)}) copy-start(f32[256,2]{0,1:T(2,128)} %param.22) | copy-start | bytes 6148
  20.5 3.5 %collective-permute-start.1 = (bf16[48,2048]{1,0:T(8,128)(2,1)S(1)}, bf16[48,2048]{1,0:T(8,128)(2,1)S(1)}, u32[]{:S(2)}, u32[]{:S(2)}) collective-permute-start(bf16[48,2048]{1,0:T(8,128)(2,1)S(1)} %get-tuple-element.38), channel_id=1, source_target_pairs={{0,1},{1,0},{2,3},{3,2},{4,5},{5,4},{6,7},{7,6},{8,9},{9,8},{10,11... | collective-permute-start | bytes 589832 | tf_op jit(solution)/shard_map/ppermute | solution.py:235
  20.5 6.0 %collective-permute-start.2 = (bf16[48,2048]{1,0:T(8,128)(2,1)S(1)}, bf16[48,2048]{1,0:T(8,128)(2,1)S(1)}, u32[]{:S(2)}, u32[]{:S(2)}) collective-permute-start(bf16[48,2048]{1,0:T(8,128)(2,1)S(1)} %get-tuple-element.39), channel_id=1, source_target_pairs={{0,2},{1,3},{2,0},{3,1},{4,6},{5,7},{6,4},{7,5},{8,10},{9,11},{10,... | collective-permute-start | bytes 589832 | tf_op jit(solution)/shard_map/ppermute | solution.py:235
  21.2 10.4 %collective-permute-start.3 = (bf16[48,2048]{1,0:T(8,128)(2,1)S(1)}, bf16[48,2048]{1,0:T(8,128)(2,1)S(1)}, u32[]{:S(2)}, u32[]{:S(2)}) collective-permute-start(bf16[48,2048]{1,0:T(8,128)(2,1)S(1)} %get-tuple-element.40), channel_id=1, source_target_pairs={{0,3},{1,2},{2,1},{3,0},{4,7},{5,6},{6,5},{7,4},{8,11},{9,10},{10,... | collective-permute-start | bytes 589832 | tf_op jit(solution)/shard_map/ppermute | solution.py:235
  22.7 11.5 %collective-permute-start.4 = (bf16[48,2048]{1,0:T(8,128)(2,1)S(1)}, bf16[48,2048]{1,0:T(8,128)(2,1)S(1)}, u32[]{:S(2)}, u32[]{:S(2)}) collective-permute-start(bf16[48,2048]{1,0:T(8,128)(2,1)S(1)} %get-tuple-element.41), channel_id=1, source_target_pairs={{0,4},{1,5},{2,6},{3,7},{4,0},{5,1},{6,2},{7,3},{8,12},{9,13},{10,... | collective-permute-start | bytes 589832 | tf_op jit(solution)/shard_map/ppermute | solution.py:235
  22.8 12.1 %collective-permute-start.5 = (bf16[48,2048]{1,0:T(8,128)(2,1)S(1)}, bf16[48,2048]{1,0:T(8,128)(2,1)S(1)}, u32[]{:S(2)}, u32[]{:S(2)}) collective-permute-start(bf16[48,2048]{1,0:T(8,128)(2,1)S(1)} %get-tuple-element.42), channel_id=1, source_target_pairs={{0,5},{1,4},{2,7},{3,6},{4,1},{5,0},{6,3},{7,2},{8,13},{9,12},{10,... | collective-permute-start | bytes 589832 | tf_op jit(solution)/shard_map/ppermute | solution.py:235
  24.7 19.4 %collective-permute-start.6 = (bf16[48,2048]{1,0:T(8,128)(2,1)}, bf16[48,2048]{1,0:T(8,128)(2,1)}, u32[]{:S(2)}, u32[]{:S(2)}) collective-permute-start(bf16[48,2048]{1,0:T(8,128)(2,1)} %get-tuple-element.43), channel_id=1, source_target_pairs={{0,6},{1,7},{2,4},{3,5},{4,2},{5,3},{6,0},{7,1},{8,14},{9,15},{10,... | collective-permute-start | bytes 589832 | tf_op jit(solution)/shard_map/ppermute | solution.py:235
  27.2 21.2 %collective-permute-start.7 = (bf16[48,2048]{1,0:T(8,128)(2,1)}, bf16[48,2048]{1,0:T(8,128)(2,1)}, u32[]{:S(2)}, u32[]{:S(2)}) collective-permute-start(bf16[48,2048]{1,0:T(8,128)(2,1)} %get-tuple-element.44), channel_id=1, source_target_pairs={{0,7},{1,6},{2,5},{3,4},{4,3},{5,2},{6,1},{7,0},{8,15},{9,14},{10,... | collective-permute-start | bytes 589832 | tf_op jit(solution)/shard_map/ppermute | solution.py:235
  32.3 16.7 %collective-permute-start.15 = (bf16[48,2048]{1,0:T(8,128)(2,1)}, bf16[48,2048]{1,0:T(8,128)(2,1)S(1)}, u32[]{:S(2)}, u32[]{:S(2)}) collective-permute-start(bf16[48,2048]{1,0:T(8,128)(2,1)} %get-tuple-element.53), channel_id=1, source_target_pairs={{0,8},{1,9},{2,10},{3,11},{4,12},{5,13},{6,14},{7,15},{8,0},{9,1},... | collective-permute-start | bytes 589832 | tf_op jit(solution)/shard_map/ppermute | solution.py:235
  34.9 33.5 %collective-permute-start.16 = (bf16[48,2048]{1,0:T(8,128)(2,1)}, bf16[48,2048]{1,0:T(8,128)(2,1)S(1)}, u32[]{:S(2)}, u32[]{:S(2)}) collective-permute-start(bf16[48,2048]{1,0:T(8,128)(2,1)} %get-tuple-element.54), channel_id=1, source_target_pairs={{0,9},{1,8},{2,11},{3,10},{4,13},{5,12},{6,15},{7,14},{8,1},{9,0},... | collective-permute-start | bytes 589832 | tf_op jit(solution)/shard_map/ppermute | solution.py:235
  35.7 37.0 %collective-permute-start.17 = (bf16[48,2048]{1,0:T(8,128)(2,1)}, bf16[48,2048]{1,0:T(8,128)(2,1)S(1)}, u32[]{:S(2)}, u32[]{:S(2)}) collective-permute-start(bf16[48,2048]{1,0:T(8,128)(2,1)} %get-tuple-element.55), channel_id=1, source_target_pairs={{0,10},{1,11},{2,8},{3,9},{4,14},{5,15},{6,12},{7,13},{8,2},{9,3},... | collective-permute-start | bytes 589832 | tf_op jit(solution)/shard_map/ppermute | solution.py:235
  44.1 62.4 %collective-permute-start.18 = (bf16[48,2048]{1,0:T(8,128)(2,1)}, bf16[48,2048]{1,0:T(8,128)(2,1)S(1)}, u32[]{:S(2)}, u32[]{:S(2)}) collective-permute-start(bf16[48,2048]{1,0:T(8,128)(2,1)} %copy-done.1), channel_id=1, source_target_pairs={{0,11},{1,10},{2,9},{3,8},{4,15},{5,14},{6,13},{7,12},{8,3},{9,2},... | collective-permute-start | bytes 589832 | tf_op jit(solution)/shard_map/ppermute | solution.py:235
  48.4 58.8 %collective-permute-start.23 = (bf16[48,2048]{1,0:T(8,128)(2,1)}, bf16[48,2048]{1,0:T(8,128)(2,1)S(1)}, u32[]{:S(2)}, u32[]{:S(2)}) collective-permute-start(bf16[48,2048]{1,0:T(8,128)(2,1)} %copy-done), channel_id=1, source_target_pairs={{0,12},{1,13},{2,14},{3,15},{4,8},{5,9},{6,10},{7,11},{8,4},{9,5},... | collective-permute-start | bytes 589832 | tf_op jit(solution)/shard_map/ppermute | solution.py:235
  49.1 59.2 %collective-permute-start.24 = (bf16[48,2048]{1,0:T(8,128)(2,1)S(1)}, bf16[48,2048]{1,0:T(8,128)(2,1)S(1)}, u32[]{:S(2)}, u32[]{:S(2)}) collective-permute-start(bf16[48,2048]{1,0:T(8,128)(2,1)S(1)} %get-tuple-element.62), channel_id=1, source_target_pairs={{0,13},{1,12},{2,15},{3,14},{4,9},{5,8},{6,11},{7,10},{8,5},{9,4},... | collective-permute-start | bytes 589832 | tf_op jit(solution)/shard_map/ppermute | solution.py:235
  68.4 40.5 %collective-permute-start.25 = (bf16[48,2048]{1,0:T(8,128)(2,1)S(1)}, bf16[48,2048]{1,0:T(8,128)(2,1)S(1)}, u32[]{:S(2)}, u32[]{:S(2)}) collective-permute-start(bf16[48,2048]{1,0:T(8,128)(2,1)S(1)} %get-tuple-element.63), channel_id=1, source_target_pairs={{0,14},{1,15},{2,12},{3,13},{4,10},{5,11},{6,8},{7,9},{8,6},{9,7},... | collective-permute-start | bytes 589832 | tf_op jit(solution)/shard_map/ppermute | solution.py:235
  72.6 41.7 %collective-permute-start.26 = (bf16[48,2048]{1,0:T(8,128)(2,1)S(1)}, bf16[48,2048]{1,0:T(8,128)(2,1)S(1)}, u32[]{:S(2)}, u32[]{:S(2)}) collective-permute-start(bf16[48,2048]{1,0:T(8,128)(2,1)S(1)} %get-tuple-element.64), channel_id=1, source_target_pairs={{0,15},{1,14},{2,13},{3,12},{4,11},{5,10},{6,9},{7,8},{8,7},{9,6},... | collective-permute-start | bytes 589832 | tf_op jit(solution)/shard_map/ppermute | solution.py:235
  106.6 28.3 %collective-permute-start.8 = (bf16[48,2048]{1,0:T(8,128)(2,1)S(1)}, bf16[48,2048]{1,0:T(8,128)(2,1)S(1)}, u32[]{:S(2)}, u32[]{:S(2)}) collective-permute-start(bf16[48,2048]{1,0:T(8,128)(2,1)S(1)} %get-tuple-element.46), channel_id=1, source_target_pairs={{0,1},{1,0},{2,3},{3,2},{4,5},{5,4},{6,7},{7,6},{8,9},{9,8},{10,11... | collective-permute-start | bytes 589832 | tf_op jit(solution)/shard_map/ppermute | solution.py:235
  107.1 30.1 %collective-permute-start.9 = (bf16[48,2048]{1,0:T(8,128)(2,1)S(1)}, bf16[48,2048]{1,0:T(8,128)(2,1)S(1)}, u32[]{:S(2)}, u32[]{:S(2)}) collective-permute-start(bf16[48,2048]{1,0:T(8,128)(2,1)S(1)} %get-tuple-element.47), channel_id=1, source_target_pairs={{0,2},{1,3},{2,0},{3,1},{4,6},{5,7},{6,4},{7,5},{8,10},{9,11},{10,... | collective-permute-start | bytes 589832 | tf_op jit(solution)/shard_map/ppermute | solution.py:235
  108.3 29.7 %collective-permute-start.10 = (bf16[48,2048]{1,0:T(8,128)(2,1)S(1)}, bf16[48,2048]{1,0:T(8,128)(2,1)S(1)}, u32[]{:S(2)}, u32[]{:S(2)}) collective-permute-start(bf16[48,2048]{1,0:T(8,128)(2,1)S(1)} %get-tuple-element.48), channel_id=1, source_target_pairs={{0,3},{1,2},{2,1},{3,0},{4,7},{5,6},{6,5},{7,4},{8,11},{9,10},{10,... | collective-permute-start | bytes 589832 | tf_op jit(solution)/shard_map/ppermute | solution.py:235
  108.9 29.1 %collective-permute-start.11 = (bf16[48,2048]{1,0:T(8,128)(2,1)S(1)}, bf16[48,2048]{1,0:T(8,128)(2,1)S(1)}, u32[]{:S(2)}, u32[]{:S(2)}) collective-permute-start(bf16[48,2048]{1,0:T(8,128)(2,1)S(1)} %get-tuple-element.49), channel_id=1, source_target_pairs={{0,4},{1,5},{2,6},{3,7},{4,0},{5,1},{6,2},{7,3},{8,12},{9,13},{10,... | collective-permute-start | bytes 589832 | tf_op jit(solution)/shard_map/ppermute | solution.py:235
  114.3 26.3 %collective-permute-start.12 = (bf16[48,2048]{1,0:T(8,128)(2,1)S(1)}, bf16[48,2048]{1,0:T(8,128)(2,1)S(1)}, u32[]{:S(2)}, u32[]{:S(2)}) collective-permute-start(bf16[48,2048]{1,0:T(8,128)(2,1)S(1)} %get-tuple-element.50), channel_id=1, source_target_pairs={{0,5},{1,4},{2,7},{3,6},{4,1},{5,0},{6,3},{7,2},{8,13},{9,12},{10,... | collective-permute-start | bytes 589832 | tf_op jit(solution)/shard_map/ppermute | solution.py:235
  134.9 27.0 %collective-permute-start.13 = (bf16[48,2048]{1,0:T(8,128)(2,1)S(1)}, bf16[48,2048]{1,0:T(8,128)(2,1)S(1)}, u32[]{:S(2)}, u32[]{:S(2)}) collective-permute-start(bf16[48,2048]{1,0:T(8,128)(2,1)S(1)} %get-tuple-element.51), channel_id=1, source_target_pairs={{0,6},{1,7},{2,4},{3,5},{4,2},{5,3},{6,0},{7,1},{8,14},{9,15},{10,... | collective-permute-start | bytes 589832 | tf_op jit(solution)/shard_map/ppermute | solution.py:235
  137.3 27.6 %collective-permute-start.14 = (bf16[48,2048]{1,0:T(8,128)(2,1)S(1)}, bf16[48,2048]{1,0:T(8,128)(2,1)S(1)}, u32[]{:S(2)}, u32[]{:S(2)}) collective-permute-start(bf16[48,2048]{1,0:T(8,128)(2,1)S(1)} %get-tuple-element.52), channel_id=1, source_target_pairs={{0,7},{1,6},{2,5},{3,4},{4,3},{5,2},{6,1},{7,0},{8,15},{9,14},{10,... | collective-permute-start | bytes 589832 | tf_op jit(solution)/shard_map/ppermute | solution.py:235
  138.0 27.2 %collective-permute-start.19 = (bf16[48,2048]{1,0:T(8,128)(2,1)S(1)}, bf16[48,2048]{1,0:T(8,128)(2,1)S(1)}, u32[]{:S(2)}, u32[]{:S(2)}) collective-permute-start(bf16[48,2048]{1,0:T(8,128)(2,1)S(1)} %get-tuple-element.57), channel_id=1, source_target_pairs={{0,8},{1,9},{2,10},{3,11},{4,12},{5,13},{6,14},{7,15},{8,0},{9,1},... | collective-permute-start | bytes 589832 | tf_op jit(solution)/shard_map/ppermute | solution.py:235
  138.0 28.6 %collective-permute-start.20 = (bf16[48,2048]{1,0:T(8,128)(2,1)S(1)}, bf16[48,2048]{1,0:T(8,128)(2,1)S(1)}, u32[]{:S(2)}, u32[]{:S(2)}) collective-permute-start(bf16[48,2048]{1,0:T(8,128)(2,1)S(1)} %get-tuple-element.58), channel_id=1, source_target_pairs={{0,9},{1,8},{2,11},{3,10},{4,13},{5,12},{6,15},{7,14},{8,1},{9,0},... | collective-permute-start | bytes 589832 | tf_op jit(solution)/shard_map/ppermute | solution.py:235
  140.6 26.9 %collective-permute-start.21 = (bf16[48,2048]{1,0:T(8,128)(2,1)S(1)}, bf16[48,2048]{1,0:T(8,128)(2,1)S(1)}, u32[]{:S(2)}, u32[]{:S(2)}) collective-permute-start(bf16[48,2048]{1,0:T(8,128)(2,1)S(1)} %get-tuple-element.59), channel_id=1, source_target_pairs={{0,10},{1,11},{2,8},{3,9},{4,14},{5,15},{6,12},{7,13},{8,2},{9,3},... | collective-permute-start | bytes 589832 | tf_op jit(solution)/shard_map/ppermute | solution.py:235
  161.9 24.3 %collective-permute-start.22 = (bf16[48,2048]{1,0:T(8,128)(2,1)S(1)}, bf16[48,2048]{1,0:T(8,128)(2,1)S(1)}, u32[]{:S(2)}, u32[]{:S(2)}) collective-permute-start(bf16[48,2048]{1,0:T(8,128)(2,1)S(1)} %get-tuple-element.60), channel_id=1, source_target_pairs={{0,11},{1,10},{2,9},{3,8},{4,15},{5,14},{6,13},{7,12},{8,3},{9,2},... | collective-permute-start | bytes 589832 | tf_op jit(solution)/shard_map/ppermute | solution.py:235
  164.8 31.4 %collective-permute-start.27 = (bf16[48,2048]{1,0:T(8,128)(2,1)S(1)}, bf16[48,2048]{1,0:T(8,128)(2,1)S(1)}, u32[]{:S(2)}, u32[]{:S(2)}) collective-permute-start(bf16[48,2048]{1,0:T(8,128)(2,1)S(1)} %get-tuple-element.65), channel_id=1, source_target_pairs={{0,12},{1,13},{2,14},{3,15},{4,8},{5,9},{6,10},{7,11},{8,4},{9,5},... | collective-permute-start | bytes 589832 | tf_op jit(solution)/shard_map/ppermute | solution.py:235
  165.1 35.7 %collective-permute-start.28 = (bf16[48,2048]{1,0:T(8,128)(2,1)S(1)}, bf16[48,2048]{1,0:T(8,128)(2,1)S(1)}, u32[]{:S(2)}, u32[]{:S(2)}) collective-permute-start(bf16[48,2048]{1,0:T(8,128)(2,1)S(1)} %get-tuple-element.66), channel_id=1, source_target_pairs={{0,13},{1,12},{2,15},{3,14},{4,9},{5,8},{6,11},{7,10},{8,5},{9,4},... | collective-permute-start | bytes 589832 | tf_op jit(solution)/shard_map/ppermute | solution.py:235
  166.6 39.0 %collective-permute-start.29 = (bf16[48,2048]{1,0:T(8,128)(2,1)S(1)}, bf16[48,2048]{1,0:T(8,128)(2,1)S(1)}, u32[]{:S(2)}, u32[]{:S(2)}) collective-permute-start(bf16[48,2048]{1,0:T(8,128)(2,1)S(1)} %get-tuple-element.67), channel_id=1, source_target_pairs={{0,14},{1,15},{2,12},{3,13},{4,10},{5,11},{6,8},{7,9},{8,6},{9,7},... | collective-permute-start | bytes 589832 | tf_op jit(solution)/shard_map/ppermute | solution.py:235
  167.5 42.4 %collective-permute-start.30 = (bf16[48,2048]{1,0:T(8,128)(2,1)S(1)}, bf16[48,2048]{1,0:T(8,128)(2,1)S(1)}, u32[]{:S(2)}, u32[]{:S(2)}) collective-permute-start(bf16[48,2048]{1,0:T(8,128)(2,1)S(1)} %get-tuple-element.68), channel_id=1, source_target_pairs={{0,15},{1,14},{2,13},{3,12},{4,11},{5,10},{6,9},{7,8},{8,7},{9,6},... | collective-permute-start | bytes 589832 | tf_op jit(solution)/shard_map/ppermute | solution.py:235
  (20 other events, 29.0 us)

commit v3 on v2

--- a/solution.py
+++ b/solution.py
@@ -12,6 +12,8 @@
 TAPS = 3
 TOP = 2
 CHUNKS = 2
+EXPERTS_VMEM = 48 * 2**20
+SMALL_VMEM = 24 * 2**20
 
 norm_eps = 1e-06
 
@@ -74,8 +76,55 @@
     return jnp.where(i < j, 1.0, 0.0).astype(jnp.bfloat16)
 
 
-def pick_body(partners, cap, routes_ref, normed_ref, *out_refs):
-    rows = normed_ref.shape[0]
+def head_body(
+    partners, cap, tail_ref, gate_b_ref, gate_c_ref, value_ref, taps_ref, ids_ref, out_weight_ref, resid_ref,
+    gains_ref, routes_ref, stream_ref, *refs,
+):
+    block_refs = refs[:partners]
+    rows_ref, ids_ext_ref, mixed_ref, proj_ref, weight_ref, picked_ref, weight_sem, block_sems = refs[partners:]
+    weight_copy = pltpu.make_async_copy(out_weight_ref, weight_ref, weight_sem)
+    weight_copy.start()
+    rows, width = gate_b_ref.shape
+    reach = TAPS - 1
+    base = rows_ref.shape[0] - rows
+
+    ids_ext_ref[base:, :] = jnp.broadcast_to(ids_ref[...], (rows, ids_ext_ref.shape[1]))
+    ids_ext_ref[base - reach : base, :] = tail_ref[:, 2 * width :].astype(jnp.float32)
+    same = [ids_ref[...] == ids_ext_ref[base - k : base - k + rows, 0:1] for k in range(1, TAPS)]
+    step = math.gcd(width, 256)
+
+    def mix(j, carry):
+        at = pl.multiple_of(j * step, step)
+        cols = pl.ds(at, step)
+        tail_gate = tail_ref[:, cols].astype(jnp.float32)
+        tail_value = tail_ref[:, pl.ds(pl.multiple_of(width + at, step), step)].astype(jnp.float32)
+        product = gate_c_ref[:, cols].astype(jnp.float32) * value_ref[:, cols].astype(jnp.float32)
+        rows_ref[base - reach : base, :] = tail_gate * tail_value
+        rows_ref[base:, :] = product
+        taps = taps_ref[:, cols].astype(jnp.float32)
+        convolved = taps[0:1] * product
+        for k in range(1, TAPS):
+            earlier = rows_ref[base - k : base - k + rows, :]
+            convolved = convolved + jnp.where(same[k - 1], taps[k : k + 1] * earlier, 0.0)
+        mixed_ref[:, cols] = (gate_b_ref[:, cols].astype(jnp.float32) * convolved).astype(jnp.bfloat16)
+        return carry
+
+    lax.fori_loop(0, width // step, mix, 0)
+    weight_copy.wait()
+    proj_ref[...] = jnp.dot(mixed_ref[...], weight_ref[...], preferred_element_type=jnp.float32).astype(jnp.bfloat16)
+
+    lines = math.gcd(rows, 32)
+
+    def normalize(j, carry):
+        at = pl.ds(pl.multiple_of(j * lines, lines), lines)
+        projected = proj_ref[at, :].astype(jnp.float32)
+        stream = resid_ref[at, :].astype(jnp.float32) + rms_scale(projected, gains_ref[0:1, :])
+        stream_ref[at, :] = stream
+        mixed_ref[at, :] = rms_scale(stream, gains_ref[1:2, :]).astype(jnp.bfloat16)
+        return carry
+
+    lax.fori_loop(0, rows // lines, normalize, 0)
+
     ids = lax.broadcasted_iota(jnp.int32, (partners, rows), 0)
     named = jnp.zeros((partners, rows), jnp.float32)
     for k in range(TOP):
@@ -83,8 +132,9 @@
     before = dot_f32(named.astype(jnp.bfloat16), earlier_than(rows, 0), ((1,), (0,)))
     slot_of = jnp.where(named > 0.0, before, -1.0).astype(jnp.bfloat16)
     group = math.gcd(partners, 4)
-    normed = normed_ref[...]
-    for first in range(0, partners, group):
+    normed = mixed_ref[...]
+    copies = []
+    for first in [*range(partners // 2, partners, group), *range(0, partners // 2, group)]:
         line = lax.broadcasted_iota(jnp.int32, (group * cap, partners), 0)
         start = (lax.broadcasted_iota(jnp.int32, (group * cap, partners), 1) - first) * cap
         mine = (line >= start) & (line < start + cap)
@@ -92,19 +142,44 @@
         spread = jnp.where(mine, 1.0, 0.0).astype(jnp.bfloat16)
         taken = dot_f32(spread, slot_of, ((1,), (0,))) == slot
         onehot = jnp.where(taken, 1.0, 0.0).astype(jnp.bfloat16)
-        picked = dot_f32(onehot, normed, ((1,), (0,))).astype(jnp.bfloat16)
-        for b in range(group):
-            out_refs[first + b][...] = picked[b * cap : (b + 1) * cap]
-
-
-def pick_blocks(partner_t, normed, partners, cap):
-    width = normed.shape[1]
+        picked_ref[first * cap : (first + group) * cap, :] = dot_f32(onehot, normed, ((1,), (0,))).astype(
+            jnp.bfloat16
+        )
+        for b in range(first, first + group):
+            copies.append(
+                pltpu.make_async_copy(picked_ref.at[b * cap : (b + 1) * cap, :], block_refs[b], block_sems.at[b])
+            )
+            copies[-1].start()
+    for copy in copies:
+        copy.wait()
+
+
+def head_call(tail, gate_b, gate_c, value, taps, doc_ids, out_weight, resid, gains, routes_t, partners, cap):
+    rows, width = gate_b.shape
+    here = pl.BlockSpec(memory_space=pltpu.VMEM)
+    far = pl.BlockSpec(memory_space=pltpu.HBM)
+    base = 8
     return pl.pallas_call(
-        functools.partial(pick_body, partners, cap),
-        out_shape=[jax.ShapeDtypeStruct((cap, width), jnp.bfloat16)] * partners,
-        compiler_params=pltpu.CompilerParams(vmem_limit_bytes=48 * 2**20),
-        name="pick",
-    )(partner_t, normed)
+        functools.partial(head_body, partners, cap),
+        in_specs=[here] * 6 + [far] + [here] * 3,
+        out_specs=[here] + [far] * partners,
+        out_shape=[
+            jax.ShapeDtypeStruct((rows, width), jnp.float32),
+            *[jax.ShapeDtypeStruct((cap, width), jnp.bfloat16)] * partners,
+        ],
+        scratch_shapes=[
+            pltpu.VMEM((base + rows, math.gcd(width, 256)), jnp.float32),
+            pltpu.VMEM((base + rows, 128), jnp.float32),
+            pltpu.VMEM((rows, width), jnp.bfloat16),
+            pltpu.VMEM((rows, width), jnp.bfloat16),
+            pltpu.VMEM((width, width), jnp.bfloat16),
+            pltpu.VMEM((partners * cap, width), jnp.bfloat16),
+            pltpu.SemaphoreType.DMA,
+            pltpu.SemaphoreType.DMA((partners,)),
+        ],
+        compiler_params=pltpu.CompilerParams(vmem_limit_bytes=EXPERTS_VMEM),
+        name="head",
+    )(tail, gate_b, gate_c, value, taps, doc_ids[:, None].astype(jnp.float32), out_weight, resid, gains, routes_t)
 
 
 def share_columns(partner, share, partners, first, count, cap):
@@ -160,8 +235,7 @@
         functools.partial(body, partners, first),
         out_shape=out,
         scratch_shapes=[pltpu.VMEM((len(blocks) * cap, width), jnp.bfloat16)],
-        compiler_params=pltpu.CompilerParams(vmem_limit_bytes=48 * 2**20),
-        name="join",
+        compiler_params=pltpu.CompilerParams(vmem_limit_bytes=SMALL_VMEM),
     )(*given, *blocks)
 
 
@@ -220,7 +294,7 @@
             bytes_accessed=6 * width * units + 4 * count * width,
         ),
         compiler_params=pltpu.CompilerParams(
-            dimension_semantics=("arbitrary",), vmem_limit_bytes=48 * 2**20
+            dimension_semantics=("arbitrary",), vmem_limit_bytes=EXPERTS_VMEM
         ),
         name="experts",
     )(*blocks, w_gate, w_up, w_down)
@@ -235,10 +309,15 @@
     return lax.ppermute(block, "sp", [(i, i ^ partner) for i in range(lax.axis_size("sp"))])
 
 
-def routed_experts(stream, normed, routes, route_weights, gain, w_gate, w_up, w_down, cap):
+def layer_by_partners(
+    resid, gate_b, gate_c, value, taps, doc_ids, out_weight, gains, routes, route_weights, w_gate, w_up, w_down, cap
+):
     partners = lax.axis_size("sp")
     partner = routes ^ lax.axis_index("sp")
-    blocks = list(pick_blocks(partner.T, normed, partners, cap))
+    tail = tail_passed(gate_c, value, doc_ids)
+    stream, *blocks = head_call(
+        tail, gate_b, gate_c, value, taps, doc_ids, out_weight, resid, gains, partner.T, partners, cap
+    )
     groups = by_partner(partners)
     for b in [*groups[0], *groups[2], *groups[1]]:
         if b > 0:
@@ -262,18 +341,24 @@
         last_body,
         partners,
         early,
-        (partner, route_weights, gain, stream, part),
+        (partner, route_weights, gains[2:3], stream, part),
         [results[b] for b in groups[2]],
         jax.ShapeDtypeStruct((rows, width), jnp.bfloat16),
     )
 
 
+def tail_passed(gate_c, value, doc_ids):
+    tok_dev = gate_c.shape[0]
+    tap_reach = TAPS - 1
+    ids_bf = jnp.broadcast_to(doc_ids[tok_dev - tap_reach :, None], (tap_reach, 128)).astype(jnp.bfloat16)
+    packed = jnp.concatenate([gate_c[tok_dev - tap_reach :], value[tok_dev - tap_reach :], ids_bf], axis=1)
+    return passed_along(packed, "sp", 1)
+
+
 def mixer_rows(gate_b, gate_c, value, taps, doc_ids):
     tok_dev, width = gate_b.shape
     tap_reach = TAPS - 1
-    ids_bf = jnp.broadcast_to(doc_ids[tok_dev - tap_reach :, None], (tap_reach, 128)).astype(jnp.bfloat16)
-    packed = jnp.concatenate([gate_c[tok_dev - tap_reach :], value[tok_dev - tap_reach :], ids_bf], axis=1)
-    got = passed_along(packed, "sp", 1).astype(jnp.float32)
+    got = tail_passed(gate_c, value, doc_ids).astype(jnp.float32)
     prev_rows = got[:, :width] * got[:, width : 2 * width]
     id_values = doc_ids.astype(jnp.float32)
     ext_ids = jnp.concatenate([got[:, 2 * width], id_values], axis=0)
@@ -311,6 +396,12 @@
     width = resid.shape[1]
     experts = lax.axis_size("sp")
     capacity = max(2, 3 * TOP * rows_blk // (2 * experts))
+    if by_partners(lax.axis_size("tp"), experts):
+        return layer_by_partners(
+            resid, gate_b, gate_c, value, taps, doc_ids, out_weight, norm_gains, routes, route_weights,
+            w_gate, w_up, w_down, capacity,
+        )
+
     offset = lax.axis_index("tp") * rows_blk
     my_routes = lax.dynamic_slice_in_dim(routes, offset, rows_blk, 0)
     my_weights = lax.dynamic_slice_in_dim(route_weights, offset, rows_blk, 0)
@@ -324,11 +415,6 @@
     ).astype(jnp.float32)
     stream = resid.astype(jnp.float32) + rms_scale(projected, norm_gains[0])
     normed = rms_scale(stream, norm_gains[1]).astype(jnp.bfloat16)
-
-    if by_partners(lax.axis_size("tp"), experts):
-        return routed_experts(
-            stream, normed, my_routes, my_weights, norm_gains[2:3], w_gate, w_up, w_down, capacity
-        )
 
     tables = route_tables(my_routes, my_weights, experts)
     edges = [capacity * c // CHUNKS for c in range(CHUNKS + 1)]

time: 213 us -> 215 us (level)
  waiting for transfers between devices: 54.3 us -> 70.7 us
  Pallas kernels: 76 us -> 91.1 us
  starting transfers between devices: 58.2 us -> 43.9 us
  matrix products: 6.53 us -> 0 us
  local copies, waits for them, and re-layouts: 13.2 us -> 8.01 us
  other arithmetic: 3.85 us -> 0.8 us
    ppermute x30, waiting for transfers between devices: 54.3 us -> 70.7 us  [crossed(): lax.ppermute(block, 'sp', [(i, i ^ partner) for i in range(lax.axis_size(...]
    pallas_call x1, Pallas kernels: 2.12 us -> 17.1 us  [head_call(): pl.pallas_call(functools.partial(head_body, partners, cap), in_specs=[her...]
    ppermute x30, starting transfers between devices: 54.5 us -> 40.2 us  [crossed(): lax.ppermute(block, 'sp', [(i, i ^ partner) for i in range(lax.axis_size(...]
    dot_general x1 -> x0, matrix products: 6.53 us -> none  [per_device(): jnp.dot(mixed, out_weight, preferred_element_type=jnp.float32)]
    unnamed x44 -> x16, local copies, waits for them, and re-layouts: 11.3 us -> 6.11 us
  transfers between devices with their start and end apart: 31 -> 31, of which waited for: 11 -> 10; matrix products, arithmetic and copies ran while one was open for 1% -> 1% of each run, Pallas kernels for 34% -> 33%
where the time goes in v3:
time: 215 us
  Pallas kernels  91.1 us (42%)
  waiting for transfers between devices  70.7 us (33%)
  starting transfers between devices  43.9 us (20%)
  local copies, waits for them, and re-layouts  8.01 us (4%)
    ppermute x30, waiting for transfers between devices, crossed(): lax.ppermute(block, 'sp', [(i, i ^ partner) for i in range(lax.axis_size(...  70.7 us
    pallas_call x3, Pallas kernels, expert_blocks(): pl.pallas_call(functools.partial(expert_body, len(blocks)), grid=(units /...  69.1 us
    ppermute x30, starting transfers between devices, crossed(): lax.ppermute(block, 'sp', [(i, i ^ partner) for i in range(lax.axis_size(...  40.2 us
    pallas_call x1, Pallas kernels, head_call(): pl.pallas_call(functools.partial(head_body, partners, cap), in_specs=[her...  17.1 us
    unnamed x16, local copies, waits for them, and re-layouts  6.11 us
    pallas_call x2, Pallas kernels, join_call(): pl.pallas_call(functools.partial(body, partners, first), out_shape=out, s...  4.91 us
  transfers between devices with their start and end apart: 31, of which 10 were waited for; matrix products, arithmetic and copies ran while one was open for 1% of the time, Pallas kernels for 33%

profile of v3, /device:TPU:11, one launch (start us, length us, event | category | flops | bytes accessed | tf_op | source)
XLA Modules:
  0.0 214.7 jit_solution(2511488711392113129)
XLA Ops:
  2.5 3.7 %collective-permute-start = (bf16[2,4224]{1,0:T(2,128)(2,1)S(1)}, bf16[2,4224]{1,0:T(2,128)(2,1)S(1)}, u32[]{:S(2)}, u32[]{:S(2)}) collective-permute-start(bf16[2,4224]{1,0:T(2,128)(2,1)S(1)} %pad_maximum_fusion), channel_id=1, source_target_pairs={{0,1},{1,2},{2,3},{3,4},{4,5},{5,6},{6,7},{7,8},{8,9},{9,10},{10,1... | collective-permute-start | bytes 50696 | tf_op jit(solution)/shard_map/ppermute | solution.py:24
  9.1 1.2 copy-done.2
  11.8 17.1 %head.1 = (f32[256,2048]{1,0:T(8,128)}, bf16[48,2048]{1,0:T(8,128)(2,1)S(1)}, bf16[48,2048]{1,0:T(8,128)(2,1)S(1)}, bf16[48,2048]{1,0:T(8,128)(2,1)S(1)}, bf16[4...) custom-call(bf16[2,4224]{1,0:T(2,128)(2,1)S(1)} %collective-permute-, ...), custom_call_target="tpu_custom_call" | custom-call | tf_op jit(solution)/shard_map/head/pallas_call | solution.py:162
  31.3 1.5 collective-permute-start.5
  33.4 2.2 %collective-permute-done.2.refs_2_ = bf16[48,2048]{1,0:T(8,128)(2,1)S(1)} collective-permute-done((bf16[48,2048]{1,0:T(8,128)(2,1)S(1)}, bf16[48,2048]{1,0:T(8,128)(2,1)S(1)}, u32[]{:S(2)}, u32[]{:S(2)}) %collective-permute-start.2) | collective-permute-done | bytes 196640 | tf_op jit(solution)/shard_map/ppermute | solution.py:309
  35.6 1.6 collective-permute-start.7
  37.3 3.2 %collective-permute-done.3.refs_3_ = bf16[48,2048]{1,0:T(8,128)(2,1)S(1)} collective-permute-done((bf16[48,2048]{1,0:T(8,128)(2,1)S(1)}, bf16[48,2048]{1,0:T(8,128)(2,1)S(1)}, u32[]{:S(2)}, u32[]{:S(2)}) %collective-permute-start.3) | collective-permute-done | bytes 196640 | tf_op jit(solution)/shard_map/ppermute | solution.py:309
  40.5 2.3 %collective-permute-start.15 = (bf16[48,2048]{1,0:T(8,128)(2,1)S(1)}, bf16[48,2048]{1,0:T(8,128)(2,1)S(1)}, u32[]{:S(2)}, u32[]{:S(2)}) collective-permute-start(bf16[48,2048]{1,0:T(8,128)(2,1)S(1)} %get-tuple-element.55), channel_id=1, source_target_pairs={{0,8},{1,9},{2,10},{3,11},{4,12},{5,13},{6,14},{7,15},{8,0},{9,1},... | collective-permute-start | bytes 589832 | tf_op jit(solution)/shard_map/ppermute | solution.py:309
  42.8 3.3 %collective-permute-start.17 = (bf16[48,2048]{1,0:T(8,128)(2,1)S(1)}, bf16[48,2048]{1,0:T(8,128)(2,1)S(1)}, u32[]{:S(2)}, u32[]{:S(2)}) collective-permute-start(bf16[48,2048]{1,0:T(8,128)(2,1)S(1)} %get-tuple-element.57), channel_id=1, source_target_pairs={{0,10},{1,11},{2,8},{3,9},{4,14},{5,15},{6,12},{7,13},{8,2},{9,3},... | collective-permute-start | bytes 589832 | tf_op jit(solution)/shard_map/ppermute | solution.py:309
  46.9 5.8 %collective-permute-done.6.refs_6_ = bf16[48,2048]{1,0:T(8,128)(2,1)} collective-permute-done((bf16[48,2048]{1,0:T(8,128)(2,1)}, bf16[48,2048]{1,0:T(8,128)(2,1)}, u32[]{:S(2)}, u32[]{:S(2)}) %collective-permute-start.6) | collective-permute-done | bytes 196640 | tf_op jit(solution)/shard_map/ppermute | solution.py:309
  52.7 4.4 %collective-permute-start.18 = (bf16[48,2048]{1,0:T(8,128)(2,1)S(1)}, bf16[48,2048]{1,0:T(8,128)(2,1)S(1)}, u32[]{:S(2)}, u32[]{:S(2)}) collective-permute-start(bf16[48,2048]{1,0:T(8,128)(2,1)S(1)} %get-tuple-element.58), channel_id=1, source_target_pairs={{0,11},{1,10},{2,9},{3,8},{4,15},{5,14},{6,13},{7,12},{8,3},{9,2},... | collective-permute-start | bytes 589832 | tf_op jit(solution)/shard_map/ppermute | solution.py:309
  57.1 1.3 collective-permute-start.23
  59.5 17.3 %collective-permute-done.16.refs_1_ = bf16[48,2048]{1,0:T(8,128)(2,1)S(1)} collective-permute-done((bf16[48,2048]{1,0:T(8,128)(2,1)S(1)}, bf16[48,2048]{1,0:T(8,128)(2,1)S(1)}, u32[]{:S(2)}, u32[]{:S(2)}) %collective-permute-start.16) | collective-permute-done | bytes 196640 | tf_op jit(solution)/shard_map/ppermute | solution.py:309
  76.7 4.2 %collective-permute-done.17.refs_2_ = bf16[48,2048]{1,0:T(8,128)(2,1)S(1)} collective-permute-done((bf16[48,2048]{1,0:T(8,128)(2,1)S(1)}, bf16[48,2048]{1,0:T(8,128)(2,1)S(1)}, u32[]{:S(2)}, u32[]{:S(2)}) %collective-permute-start.17) | collective-permute-done | bytes 196640 | tf_op jit(solution)/shard_map/ppermute | solution.py:309
  81.4 27.7 %experts.3 = (bf16[48,2048]{1,0:T(8,128)(2,1)S(1)}, bf16[48,2048]{1,0:T(8,128)(2,1)S(1)}, bf16[48,2048]{1,0:T(8,128)(2,1)S(1)}, bf16[48,2048]{1,0:T(8,128)(2,1)S...) custom-call(bf16[48,2048]{1,0:T(8,128)(2,1)S(1)} %get-tuple-element., ...), custom_call_target="tpu_custom_call" | custom-call | flops 19327352832 | bytes 53477376 | tf_op jit(solution)/shard_map/experts/pallas_call | solution.py:279
  109.2 1.6 collective-permute-start.10
  110.8 4.6 %collective-permute-start.11 = (bf16[48,2048]{1,0:T(8,128)(2,1)S(1)}, bf16[48,2048]{1,0:T(8,128)(2,1)S(1)}, u32[]{:S(2)}, u32[]{:S(2)}) collective-permute-start(bf16[48,2048]{1,0:T(8,128)(2,1)S(1)} %get-tuple-element.51), channel_id=1, source_target_pairs={{0,4},{1,5},{2,6},{3,7},{4,0},{5,1},{6,2},{7,3},{8,12},{9,13},{10,... | collective-permute-start | bytes 589832 | tf_op jit(solution)/shard_map/ppermute | solution.py:309
  116.3 1.7 collective-permute-start.13
  118.0 1.2 collective-permute-start.14
  119.3 20.6 %experts.4 = (bf16[48,2048]{1,0:T(8,128)(2,1)S(1)}, bf16[48,2048]{1,0:T(8,128)(2,1)S(1)}, bf16[48,2048]{1,0:T(8,128)(2,1)S(1)}, bf16[48,2048]{1,0:T(8,128)(2,1)S(1)}) custom-call(bf16[48,2048]{1,0:T(8,128)(2,1)S(1)} %collective-permute-done.15.refs_0_, bf16[48,2048]{1,0:T(8,128)(2,1)S(1)} %collective-permute-done.16.refs_1_, ...), custom_call_target="tpu_custom_call" | custom-call | flops 9663676416 | bytes 51904512 | tf_op jit(solution)/shard_map/experts/pallas_call | solution.py:279
  140.5 3.1 %collective-permute-start.20 = (bf16[48,2048]{1,0:T(8,128)(2,1)S(1)}, bf16[48,2048]{1,0:T(8,128)(2,1)S(1)}, u32[]{:S(2)}, u32[]{:S(2)}) collective-permute-start(bf16[48,2048]{1,0:T(8,128)(2,1)S(1)} %get-tuple-element.60), channel_id=1, source_target_pairs={{0,9},{1,8},{2,11},{3,10},{4,13},{5,12},{6,15},{7,14},{8,1},{9,0},... | collective-permute-start | bytes 589832 | tf_op jit(solution)/shard_map/ppermute | solution.py:309
  144.3 20.8 %experts.5 = (bf16[48,2048]{1,0:T(8,128)(2,1)S(1)}, bf16[48,2048]{1,0:T(8,128)(2,1)S(1)}, bf16[48,2048]{1,0:T(8,128)(2,1)S(1)}, bf16[48,2048]{1,0:T(8,128)(2,1)S(1)}) custom-call(bf16[48,2048]{1,0:T(8,128)(2,1)S(1)} %collective-permute-done.23.refs_0_, bf16[48,2048]{1,0:T(8,128)(2,1)S(1)} %collective-permute-done.24.refs_1_, ...), custom_call_target="tpu_custom_call" | custom-call | flops 9663676416 | bytes 51904512 | tf_op jit(solution)/shard_map/experts/pallas_call | solution.py:279
  165.1 2.4 %collective-permute-start.22 = (bf16[48,2048]{1,0:T(8,128)(2,1)S(1)}, bf16[48,2048]{1,0:T(8,128)(2,1)S(1)}, u32[]{:S(2)}, u32[]{:S(2)}) collective-permute-start(bf16[48,2048]{1,0:T(8,128)(2,1)S(1)} %get-tuple-element.62), channel_id=1, source_target_pairs={{0,11},{1,10},{2,9},{3,8},{4,15},{5,14},{6,13},{7,12},{8,3},{9,2},... | collective-permute-start | bytes 589832 | tf_op jit(solution)/shard_map/ppermute | solution.py:309
  168.1 1.7 collective-permute-start.28
  170.4 1.4 collective-permute-start.30
  171.9 20.5 %collective-permute-done.22.refs_11_ = bf16[48,2048]{1,0:T(8,128)(2,1)S(1)} collective-permute-done((bf16[48,2048]{1,0:T(8,128)(2,1)S(1)}, bf16[48,2048]{1,0:T(8,128)(2,1)S(1)}, u32[]{:S(2)}, u32[]{:S(2)}) %collective-permute-start.22) | collective-permute-done | bytes 196640 | tf_op jit(solution)/shard_map/ppermute | solution.py:309
  192.4 2.4 %shard_map.127.part_ref = f32[256,2048]{1,0:T(8,128)S(1)} custom-call(s32[256,2]{1,0:T(8,128)S(1)} %broadcast_xor_fusion.partner_ref, f32[256,2]{1,0:T(8,128)S(1)} %copy.22.share_ref, bf16[48,2048]{1,0:T(8,128)(2,1)S(1)} %get-tuple-element.47.refs_0_, bf16[48,2048]{1,0:T(8,128)(2,1)S(1)} %collective-permute-done.8.refs_1_, ...), custom_call_target="tpu_custom_call" | custom-call | tf_op jit(solution)/shard_map/pallas_call | solution.py:234
  194.8 3.9 %collective-permute-done.27.refs_0_ = bf16[48,2048]{1,0:T(8,128)(2,1)S(1)} collective-permute-done((bf16[48,2048]{1,0:T(8,128)(2,1)S(1)}, bf16[48,2048]{1,0:T(8,128)(2,1)S(1)}, u32[]{:S(2)}, u32[]{:S(2)}) %collective-permute-start.27) | collective-permute-done | bytes 196640 | tf_op jit(solution)/shard_map/ppermute | solution.py:309
  198.7 4.2 %collective-permute-done.28.refs_1_ = bf16[48,2048]{1,0:T(8,128)(2,1)S(1)} collective-permute-done((bf16[48,2048]{1,0:T(8,128)(2,1)S(1)}, bf16[48,2048]{1,0:T(8,128)(2,1)S(1)}, u32[]{:S(2)}, u32[]{:S(2)}) %collective-permute-start.28) | collective-permute-done | bytes 196640 | tf_op jit(solution)/shard_map/ppermute | solution.py:309
  202.9 5.1 %collective-permute-done.29.refs_2_ = bf16[48,2048]{1,0:T(8,128)(2,1)S(1)} collective-permute-done((bf16[48,2048]{1,0:T(8,128)(2,1)S(1)}, bf16[48,2048]{1,0:T(8,128)(2,1)S(1)}, u32[]{:S(2)}, u32[]{:S(2)}) %collective-permute-start.29) | collective-permute-done | bytes 196640 | tf_op jit(solution)/shard_map/ppermute | solution.py:309
  208.0 4.2 %collective-permute-done.30.refs_3_ = bf16[48,2048]{1,0:T(8,128)(2,1)S(1)} collective-permute-done((bf16[48,2048]{1,0:T(8,128)(2,1)S(1)}, bf16[48,2048]{1,0:T(8,128)(2,1)S(1)}, u32[]{:S(2)}, u32[]{:S(2)}) %collective-permute-start.30) | collective-permute-done | bytes 196640 | tf_op jit(solution)/shard_map/ppermute | solution.py:309
  212.2 2.5 %shard_map.128 = bf16[256,2048]{1,0:T(8,128)(2,1)} custom-call(s32[256,2]{1,0:T(8,128)S(1)} %broadcast_xor_fusion.partner_ref, f32[256,2]{1,0:T(8,128)S(1)} %copy.22.share_ref, f32[1,2048]{1,0:T(1,128)S(1)} %slice.13.gain_ref, f32[256,2048]{1,0:T(8,128)S(1)} %copy-done, f32[256,2048]{1,0:T(8,128)S(1)} %shard_map.127.part_ref, ...), custom_call_target="tpu_custom_call" | custom-call | tf_op jit(solution)/shard_map/pallas_call | solution.py:234
  (63 shorter events, 15.8 us)
Async XLA Ops:
  2.5 5.4 %collective-permute-start = (bf16[2,4224]{1,0:T(2,128)(2,1)S(1)}, bf16[2,4224]{1,0:T(2,128)(2,1)S(1)}, u32[]{:S(2)}, u32[]{:S(2)}) collective-permute-start(bf16[2,4224]{1,0:T(2,128)(2,1)S(1)} %pad_maximum_fusion), channel_id=1, source_target_pairs={{0,1},{1,2},{2,3},{3,4},{4,5},{5,6},{6,7},{7,8},{8,9},{9,10},{10,1... | collective-permute-start | bytes 50696 | tf_op jit(solution)/shard_map/ppermute | solution.py:24
  28.9 3.9 %collective-permute-start.1 = (bf16[48,2048]{1,0:T(8,128)(2,1)S(1)}, bf16[48,2048]{1,0:T(8,128)(2,1)S(1)}, u32[]{:S(2)}, u32[]{:S(2)}) collective-permute-start(bf16[48,2048]{1,0:T(8,128)(2,1)S(1)} %get-tuple-element.40), channel_id=1, source_target_pairs={{0,1},{1,0},{2,3},{3,2},{4,5},{5,4},{6,7},{7,6},{8,9},{9,8},{10,11... | collective-permute-start | bytes 589832 | tf_op jit(solution)/shard_map/ppermute | solution.py:309
  29.3 6.3 %collective-permute-start.2 = (bf16[48,2048]{1,0:T(8,128)(2,1)S(1)}, bf16[48,2048]{1,0:T(8,128)(2,1)S(1)}, u32[]{:S(2)}, u32[]{:S(2)}) collective-permute-start(bf16[48,2048]{1,0:T(8,128)(2,1)S(1)} %get-tuple-element.41), channel_id=1, source_target_pairs={{0,2},{1,3},{2,0},{3,1},{4,6},{5,7},{6,4},{7,5},{8,10},{9,11},{10,... | collective-permute-start | bytes 589832 | tf_op jit(solution)/shard_map/ppermute | solution.py:309
  30.5 10.0 %collective-permute-start.3 = (bf16[48,2048]{1,0:T(8,128)(2,1)S(1)}, bf16[48,2048]{1,0:T(8,128)(2,1)S(1)}, u32[]{:S(2)}, u32[]{:S(2)}) collective-permute-start(bf16[48,2048]{1,0:T(8,128)(2,1)S(1)} %get-tuple-element.42), channel_id=1, source_target_pairs={{0,3},{1,2},{2,1},{3,0},{4,7},{5,6},{6,5},{7,4},{8,11},{9,10},{10,... | collective-permute-start | bytes 589832 | tf_op jit(solution)/shard_map/ppermute | solution.py:309
  31.1 11.6 %collective-permute-start.4 = (bf16[48,2048]{1,0:T(8,128)(2,1)S(1)}, bf16[48,2048]{1,0:T(8,128)(2,1)S(1)}, u32[]{:S(2)}, u32[]{:S(2)}) collective-permute-start(bf16[48,2048]{1,0:T(8,128)(2,1)S(1)} %get-tuple-element.43), channel_id=1, source_target_pairs={{0,4},{1,5},{2,6},{3,7},{4,0},{5,1},{6,2},{7,3},{8,12},{9,13},{10,... | collective-permute-start | bytes 589832 | tf_op jit(solution)/shard_map/ppermute | solution.py:309
  31.3 11.5 %collective-permute-start.5 = (bf16[48,2048]{1,0:T(8,128)(2,1)S(1)}, bf16[48,2048]{1,0:T(8,128)(2,1)S(1)}, u32[]{:S(2)}, u32[]{:S(2)}) collective-permute-start(bf16[48,2048]{1,0:T(8,128)(2,1)S(1)} %get-tuple-element.44), channel_id=1, source_target_pairs={{0,5},{1,4},{2,7},{3,6},{4,1},{5,0},{6,3},{7,2},{8,13},{9,12},{10,... | collective-permute-start | bytes 589832 | tf_op jit(solution)/shard_map/ppermute | solution.py:309
  32.8 19.8 %collective-permute-start.6 = (bf16[48,2048]{1,0:T(8,128)(2,1)}, bf16[48,2048]{1,0:T(8,128)(2,1)}, u32[]{:S(2)}, u32[]{:S(2)}) collective-permute-start(bf16[48,2048]{1,0:T(8,128)(2,1)} %get-tuple-element.45), channel_id=1, source_target_pairs={{0,6},{1,7},{2,4},{3,5},{4,2},{5,3},{6,0},{7,1},{8,14},{9,15},{10,... | collective-permute-start | bytes 589832 | tf_op jit(solution)/shard_map/ppermute | solution.py:309
  35.6 21.4 %collective-permute-start.7 = (bf16[48,2048]{1,0:T(8,128)(2,1)}, bf16[48,2048]{1,0:T(8,128)(2,1)}, u32[]{:S(2)}, u32[]{:S(2)}) collective-permute-start(bf16[48,2048]{1,0:T(8,128)(2,1)} %get-tuple-element.46), channel_id=1, source_target_pairs={{0,7},{1,6},{2,5},{3,4},{4,3},{5,2},{6,1},{7,0},{8,15},{9,14},{10,... | collective-permute-start | bytes 589832 | tf_op jit(solution)/shard_map/ppermute | solution.py:309
  40.5 17.9 %collective-permute-start.15 = (bf16[48,2048]{1,0:T(8,128)(2,1)S(1)}, bf16[48,2048]{1,0:T(8,128)(2,1)S(1)}, u32[]{:S(2)}, u32[]{:S(2)}) collective-permute-start(bf16[48,2048]{1,0:T(8,128)(2,1)S(1)} %get-tuple-element.55), channel_id=1, source_target_pairs={{0,8},{1,9},{2,10},{3,11},{4,12},{5,13},{6,14},{7,15},{8,0},{9,1},... | collective-permute-start | bytes 589832 | tf_op jit(solution)/shard_map/ppermute | solution.py:309
  42.8 33.9 %collective-permute-start.16 = (bf16[48,2048]{1,0:T(8,128)(2,1)S(1)}, bf16[48,2048]{1,0:T(8,128)(2,1)S(1)}, u32[]{:S(2)}, u32[]{:S(2)}) collective-permute-start(bf16[48,2048]{1,0:T(8,128)(2,1)S(1)} %get-tuple-element.56), channel_id=1, source_target_pairs={{0,9},{1,8},{2,11},{3,10},{4,13},{5,12},{6,15},{7,14},{8,1},{9,0},... | collective-permute-start | bytes 589832 | tf_op jit(solution)/shard_map/ppermute | solution.py:309
  42.8 38.1 %collective-permute-start.17 = (bf16[48,2048]{1,0:T(8,128)(2,1)S(1)}, bf16[48,2048]{1,0:T(8,128)(2,1)S(1)}, u32[]{:S(2)}, u32[]{:S(2)}) collective-permute-start(bf16[48,2048]{1,0:T(8,128)(2,1)S(1)} %get-tuple-element.57), channel_id=1, source_target_pairs={{0,10},{1,11},{2,8},{3,9},{4,14},{5,15},{6,12},{7,13},{8,2},{9,3},... | collective-permute-start | bytes 589832 | tf_op jit(solution)/shard_map/ppermute | solution.py:309
  52.7 56.5 %collective-permute-start.18 = (bf16[48,2048]{1,0:T(8,128)(2,1)S(1)}, bf16[48,2048]{1,0:T(8,128)(2,1)S(1)}, u32[]{:S(2)}, u32[]{:S(2)}) collective-permute-start(bf16[48,2048]{1,0:T(8,128)(2,1)S(1)} %get-tuple-element.58), channel_id=1, source_target_pairs={{0,11},{1,10},{2,9},{3,8},{4,15},{5,14},{6,13},{7,12},{8,3},{9,2},... | collective-permute-start | bytes 589832 | tf_op jit(solution)/shard_map/ppermute | solution.py:309
  57.1 53.7 %collective-permute-start.23 = (bf16[48,2048]{1,0:T(8,128)(2,1)S(1)}, bf16[48,2048]{1,0:T(8,128)(2,1)S(1)}, u32[]{:S(2)}, u32[]{:S(2)}) collective-permute-start(bf16[48,2048]{1,0:T(8,128)(2,1)S(1)} %get-tuple-element.63), channel_id=1, source_target_pairs={{0,12},{1,13},{2,14},{3,15},{4,8},{5,9},{6,10},{7,11},{8,4},{9,5},... | collective-permute-start | bytes 589832 | tf_op jit(solution)/shard_map/ppermute | solution.py:309
  58.3 57.0 %collective-permute-start.24 = (bf16[48,2048]{1,0:T(8,128)(2,1)S(1)}, bf16[48,2048]{1,0:T(8,128)(2,1)S(1)}, u32[]{:S(2)}, u32[]{:S(2)}) collective-permute-start(bf16[48,2048]{1,0:T(8,128)(2,1)S(1)} %get-tuple-element.64), channel_id=1, source_target_pairs={{0,13},{1,12},{2,15},{3,14},{4,9},{5,8},{6,11},{7,10},{8,5},{9,4},... | collective-permute-start | bytes 589832 | tf_op jit(solution)/shard_map/ppermute | solution.py:309
  76.7 39.6 %collective-permute-start.25 = (bf16[48,2048]{1,0:T(8,128)(2,1)S(1)}, bf16[48,2048]{1,0:T(8,128)(2,1)S(1)}, u32[]{:S(2)}, u32[]{:S(2)}) collective-permute-start(bf16[48,2048]{1,0:T(8,128)(2,1)S(1)} %get-tuple-element.65), channel_id=1, source_target_pairs={{0,14},{1,15},{2,12},{3,13},{4,10},{5,11},{6,8},{7,9},{8,6},{9,7},... | collective-permute-start | bytes 589832 | tf_op jit(solution)/shard_map/ppermute | solution.py:309
  80.9 37.1 %collective-permute-start.26 = (bf16[48,2048]{1,0:T(8,128)(2,1)S(1)}, bf16[48,2048]{1,0:T(8,128)(2,1)S(1)}, u32[]{:S(2)}, u32[]{:S(2)}) collective-permute-start(bf16[48,2048]{1,0:T(8,128)(2,1)S(1)} %get-tuple-element.66), channel_id=1, source_target_pairs={{0,15},{1,14},{2,13},{3,12},{4,11},{5,10},{6,9},{7,8},{8,7},{9,6},... | collective-permute-start | bytes 589832 | tf_op jit(solution)/shard_map/ppermute | solution.py:309
  109.2 30.7 %collective-permute-start.10 = (bf16[48,2048]{1,0:T(8,128)(2,1)S(1)}, bf16[48,2048]{1,0:T(8,128)(2,1)S(1)}, u32[]{:S(2)}, u32[]{:S(2)}) collective-permute-start(bf16[48,2048]{1,0:T(8,128)(2,1)S(1)} %get-tuple-element.50), channel_id=1, source_target_pairs={{0,3},{1,2},{2,1},{3,0},{4,7},{5,6},{6,5},{7,4},{8,11},{9,10},{10,... | collective-permute-start | bytes 589832 | tf_op jit(solution)/shard_map/ppermute | solution.py:309
  110.8 29.2 %collective-permute-start.11 = (bf16[48,2048]{1,0:T(8,128)(2,1)S(1)}, bf16[48,2048]{1,0:T(8,128)(2,1)S(1)}, u32[]{:S(2)}, u32[]{:S(2)}) collective-permute-start(bf16[48,2048]{1,0:T(8,128)(2,1)S(1)} %get-tuple-element.51), channel_id=1, source_target_pairs={{0,4},{1,5},{2,6},{3,7},{4,0},{5,1},{6,2},{7,3},{8,12},{9,13},{10,... | collective-permute-start | bytes 589832 | tf_op jit(solution)/shard_map/ppermute | solution.py:309
  115.4 25.0 %collective-permute-start.12 = (bf16[48,2048]{1,0:T(8,128)(2,1)S(1)}, bf16[48,2048]{1,0:T(8,128)(2,1)S(1)}, u32[]{:S(2)}, u32[]{:S(2)}) collective-permute-start(bf16[48,2048]{1,0:T(8,128)(2,1)S(1)} %get-tuple-element.52), channel_id=1, source_target_pairs={{0,5},{1,4},{2,7},{3,6},{4,1},{5,0},{6,3},{7,2},{8,13},{9,12},{10,... | collective-permute-start | bytes 589832 | tf_op jit(solution)/shard_map/ppermute | solution.py:309
  116.3 24.2 %collective-permute-start.13 = (bf16[48,2048]{1,0:T(8,128)(2,1)S(1)}, bf16[48,2048]{1,0:T(8,128)(2,1)S(1)}, u32[]{:S(2)}, u32[]{:S(2)}) collective-permute-start(bf16[48,2048]{1,0:T(8,128)(2,1)S(1)} %get-tuple-element.53), channel_id=1, source_target_pairs={{0,6},{1,7},{2,4},{3,5},{4,2},{5,3},{6,0},{7,1},{8,14},{9,15},{10,... | collective-permute-start | bytes 589832 | tf_op jit(solution)/shard_map/ppermute | solution.py:309
  118.0 25.6 %collective-permute-start.14 = (bf16[48,2048]{1,0:T(8,128)(2,1)S(1)}, bf16[48,2048]{1,0:T(8,128)(2,1)S(1)}, u32[]{:S(2)}, u32[]{:S(2)}) collective-permute-start(bf16[48,2048]{1,0:T(8,128)(2,1)S(1)} %get-tuple-element.54), channel_id=1, source_target_pairs={{0,7},{1,6},{2,5},{3,4},{4,3},{5,2},{6,1},{7,0},{8,15},{9,14},{10,... | collective-permute-start | bytes 589832 | tf_op jit(solution)/shard_map/ppermute | solution.py:309
  139.9 25.2 %collective-permute-start.8 = (bf16[48,2048]{1,0:T(8,128)(2,1)S(1)}, bf16[48,2048]{1,0:T(8,128)(2,1)S(1)}, u32[]{:S(2)}, u32[]{:S(2)}) collective-permute-start(bf16[48,2048]{1,0:T(8,128)(2,1)S(1)} %get-tuple-element.48), channel_id=1, source_target_pairs={{0,1},{1,0},{2,3},{3,2},{4,5},{5,4},{6,7},{7,6},{8,9},{9,8},{10,11... | collective-permute-start | bytes 589832 | tf_op jit(solution)/shard_map/ppermute | solution.py:309
  140.0 27.5 %collective-permute-start.9 = (bf16[48,2048]{1,0:T(8,128)(2,1)S(1)}, bf16[48,2048]{1,0:T(8,128)(2,1)S(1)}, u32[]{:S(2)}, u32[]{:S(2)}) collective-permute-start(bf16[48,2048]{1,0:T(8,128)(2,1)S(1)} %get-tuple-element.49), channel_id=1, source_target_pairs={{0,2},{1,3},{2,0},{3,1},{4,6},{5,7},{6,4},{7,5},{8,10},{9,11},{10,... | collective-permute-start | bytes 589832 | tf_op jit(solution)/shard_map/ppermute | solution.py:309
  140.4 27.7 %collective-permute-start.19 = (bf16[48,2048]{1,0:T(8,128)(2,1)S(1)}, bf16[48,2048]{1,0:T(8,128)(2,1)S(1)}, u32[]{:S(2)}, u32[]{:S(2)}) collective-permute-start(bf16[48,2048]{1,0:T(8,128)(2,1)S(1)} %get-tuple-element.59), channel_id=1, source_target_pairs={{0,8},{1,9},{2,10},{3,11},{4,12},{5,13},{6,14},{7,15},{8,0},{9,1},... | collective-permute-start | bytes 589832 | tf_op jit(solution)/shard_map/ppermute | solution.py:309
  140.5 29.2 %collective-permute-start.20 = (bf16[48,2048]{1,0:T(8,128)(2,1)S(1)}, bf16[48,2048]{1,0:T(8,128)(2,1)S(1)}, u32[]{:S(2)}, u32[]{:S(2)}) collective-permute-start(bf16[48,2048]{1,0:T(8,128)(2,1)S(1)} %get-tuple-element.60), channel_id=1, source_target_pairs={{0,9},{1,8},{2,11},{3,10},{4,13},{5,12},{6,15},{7,14},{8,1},{9,0},... | collective-permute-start | bytes 589832 | tf_op jit(solution)/shard_map/ppermute | solution.py:309
  143.6 68.6 %copy-start = (f32[256,2048]{1,0:T(8,128)S(1)}, f32[256,2048]{1,0:T(8,128)}, u32[]{:S(2)}) copy-start(f32[256,2048]{1,0:T(8,128)} %get-tuple-element.38.stream_ref) | copy-start | bytes 6291460
  143.6 26.9 %collective-permute-start.21 = (bf16[48,2048]{1,0:T(8,128)(2,1)S(1)}, bf16[48,2048]{1,0:T(8,128)(2,1)S(1)}, u32[]{:S(2)}, u32[]{:S(2)}) collective-permute-start(bf16[48,2048]{1,0:T(8,128)(2,1)S(1)} %get-tuple-element.61), channel_id=1, source_target_pairs={{0,10},{1,11},{2,8},{3,9},{4,14},{5,15},{6,12},{7,13},{8,2},{9,3},... | collective-permute-start | bytes 589832 | tf_op jit(solution)/shard_map/ppermute | solution.py:309
  165.1 27.3 %collective-permute-start.22 = (bf16[48,2048]{1,0:T(8,128)(2,1)S(1)}, bf16[48,2048]{1,0:T(8,128)(2,1)S(1)}, u32[]{:S(2)}, u32[]{:S(2)}) collective-permute-start(bf16[48,2048]{1,0:T(8,128)(2,1)S(1)} %get-tuple-element.62), channel_id=1, source_target_pairs={{0,11},{1,10},{2,9},{3,8},{4,15},{5,14},{6,13},{7,12},{8,3},{9,2},... | collective-permute-start | bytes 589832 | tf_op jit(solution)/shard_map/ppermute | solution.py:309
  167.5 31.2 %collective-permute-start.27 = (bf16[48,2048]{1,0:T(8,128)(2,1)S(1)}, bf16[48,2048]{1,0:T(8,128)(2,1)S(1)}, u32[]{:S(2)}, u32[]{:S(2)}) collective-permute-start(bf16[48,2048]{1,0:T(8,128)(2,1)S(1)} %get-tuple-element.67), channel_id=1, source_target_pairs={{0,12},{1,13},{2,14},{3,15},{4,8},{5,9},{6,10},{7,11},{8,4},{9,5},... | collective-permute-start | bytes 589832 | tf_op jit(solution)/shard_map/ppermute | solution.py:309
  168.1 34.8 %collective-permute-start.28 = (bf16[48,2048]{1,0:T(8,128)(2,1)S(1)}, bf16[48,2048]{1,0:T(8,128)(2,1)S(1)}, u32[]{:S(2)}, u32[]{:S(2)}) collective-permute-start(bf16[48,2048]{1,0:T(8,128)(2,1)S(1)} %get-tuple-element.68), channel_id=1, source_target_pairs={{0,13},{1,12},{2,15},{3,14},{4,9},{5,8},{6,11},{7,10},{8,5},{9,4},... | collective-permute-start | bytes 589832 | tf_op jit(solution)/shard_map/ppermute | solution.py:309
  169.8 38.3 %collective-permute-start.29 = (bf16[48,2048]{1,0:T(8,128)(2,1)S(1)}, bf16[48,2048]{1,0:T(8,128)(2,1)S(1)}, u32[]{:S(2)}, u32[]{:S(2)}) collective-permute-start(bf16[48,2048]{1,0:T(8,128)(2,1)S(1)} %get-tuple-element.69), channel_id=1, source_target_pairs={{0,14},{1,15},{2,12},{3,13},{4,10},{5,11},{6,8},{7,9},{8,6},{9,7},... | collective-permute-start | bytes 589832 | tf_op jit(solution)/shard_map/ppermute | solution.py:309
  170.4 41.8 %collective-permute-start.30 = (bf16[48,2048]{1,0:T(8,128)(2,1)S(1)}, bf16[48,2048]{1,0:T(8,128)(2,1)S(1)}, u32[]{:S(2)}, u32[]{:S(2)}) collective-permute-start(bf16[48,2048]{1,0:T(8,128)(2,1)S(1)} %get-tuple-element.70), channel_id=1, source_target_pairs={{0,15},{1,14},{2,13},{3,12},{4,11},{5,10},{6,9},{7,8},{8,7},{9,6},... | collective-permute-start | bytes 589832 | tf_op jit(solution)/shard_map/ppermute | solution.py:309
  (6 other events, 32.9 us)

commit v4 on v2

--- a/solution.py
+++ b/solution.py
@@ -12,6 +12,8 @@
 TAPS = 3
 TOP = 2
 CHUNKS = 2
+EXPERTS_VMEM = 48 * 2**20
+SMALL_VMEM = 24 * 2**20
 
 norm_eps = 1e-06
 
@@ -74,7 +76,8 @@
     return jnp.where(i < j, 1.0, 0.0).astype(jnp.bfloat16)
 
 
-def pick_body(partners, cap, routes_ref, normed_ref, *out_refs):
+def pick_body(partners, cap, routes_ref, normed_ref, *refs):
+    block_refs, (picked_ref, sems) = refs[:partners], refs[partners:]
     rows = normed_ref.shape[0]
     ids = lax.broadcasted_iota(jnp.int32, (partners, rows), 0)
     named = jnp.zeros((partners, rows), jnp.float32)
@@ -84,6 +87,7 @@
     slot_of = jnp.where(named > 0.0, before, -1.0).astype(jnp.bfloat16)
     group = math.gcd(partners, 4)
     normed = normed_ref[...]
+    copies = []
     for first in range(0, partners, group):
         line = lax.broadcasted_iota(jnp.int32, (group * cap, partners), 0)
         start = (lax.broadcasted_iota(jnp.int32, (group * cap, partners), 1) - first) * cap
@@ -93,16 +97,24 @@
         taken = dot_f32(spread, slot_of, ((1,), (0,))) == slot
         onehot = jnp.where(taken, 1.0, 0.0).astype(jnp.bfloat16)
         picked = dot_f32(onehot, normed, ((1,), (0,))).astype(jnp.bfloat16)
-        for b in range(group):
-            out_refs[first + b][...] = picked[b * cap : (b + 1) * cap]
+        picked_ref[first * cap : (first + group) * cap, :] = picked
+        for b in range(first, first + group):
+            copies.append(
+                pltpu.make_async_copy(picked_ref.at[b * cap : (b + 1) * cap, :], block_refs[b], sems.at[b])
+            )
+            copies[-1].start()
+    for copy in copies:
+        copy.wait()
 
 
 def pick_blocks(partner_t, normed, partners, cap):
     width = normed.shape[1]
     return pl.pallas_call(
         functools.partial(pick_body, partners, cap),
-        out_shape=[jax.ShapeDtypeStruct((cap, width), jnp.bfloat16)] * partners,
-        compiler_params=pltpu.CompilerParams(vmem_limit_bytes=48 * 2**20),
+        out_specs=[pl.BlockSpec(memory_space=pltpu.HBM)] * partners,
+        out_shape=[pltpu.HBM((cap, width), jnp.bfloat16)] * partners,
+        scratch_shapes=[pltpu.VMEM((partners * cap, width), jnp.bfloat16), pltpu.SemaphoreType.DMA((partners,))],
+        compiler_params=pltpu.CompilerParams(vmem_limit_bytes=SMALL_VMEM),
         name="pick",
     )(partner_t, normed)
 
@@ -160,8 +172,7 @@
         functools.partial(body, partners, first),
         out_shape=out,
         scratch_shapes=[pltpu.VMEM((len(blocks) * cap, width), jnp.bfloat16)],
-        compiler_params=pltpu.CompilerParams(vmem_limit_bytes=48 * 2**20),
-        name="join",
+        compiler_params=pltpu.CompilerParams(vmem_limit_bytes=SMALL_VMEM),
     )(*given, *blocks)
 
 
@@ -199,7 +210,7 @@
 def expert_blocks(blocks, w_gate, w_up, w_down):
     cap, width = blocks[0].shape
     units = w_gate.shape[2]
-    block = math.gcd(units, 512)
+    block = math.gcd(units, 1024)
     count = len(blocks) * cap
     whole = pl.BlockSpec((cap, width), lambda j: (0, 0))
     return pl.pallas_call(
@@ -220,7 +231,7 @@
             bytes_accessed=6 * width * units + 4 * count * width,
         ),
         compiler_params=pltpu.CompilerParams(
-            dimension_semantics=("arbitrary",), vmem_limit_bytes=48 * 2**20
+            dimension_semantics=("arbitrary",), vmem_limit_bytes=EXPERTS_VMEM
         ),
         name="experts",
     )(*blocks, w_gate, w_up, w_down)
@@ -228,7 +239,7 @@
 
 def by_partner(partners):
     half, quarter = partners // 2, partners // 4
-    return [range(half, half + quarter), range(half), range(half + quarter, partners)]
+    return range(quarter), range(quarter, half), range(half, half + quarter), range(half + quarter, partners)
 
 
 def crossed(block, partner):
@@ -239,17 +250,17 @@
     partners = lax.axis_size("sp")
     partner = routes ^ lax.axis_index("sp")
     blocks = list(pick_blocks(partner.T, normed, partners, cap))
-    groups = by_partner(partners)
-    for b in [*groups[0], *groups[2], *groups[1]]:
+    same, near, far_a, far_b = by_partner(partners)
+    for b in range(partners):
         if b > 0:
             blocks[b] = crossed(blocks[b], b)
     results = {}
-    for group in groups:
+    for group in [same, far_a, [*near, *far_b]]:
         worked = expert_blocks([blocks[b] for b in group], w_gate, w_up, w_down)
         for b, block in zip(group, worked):
             results[b] = crossed(block, b) if b > 0 else block
     rows, width = stream.shape
-    early = groups[2][0]
+    early = far_b[0]
     part = join_call(
         join_body,
         partners,
@@ -263,17 +274,23 @@
         partners,
         early,
         (partner, route_weights, gain, stream, part),
-        [results[b] for b in groups[2]],
+        [results[b] for b in far_b],
         jax.ShapeDtypeStruct((rows, width), jnp.bfloat16),
     )
+
+
+def tail_passed(gate_c, value, doc_ids):
+    tok_dev = gate_c.shape[0]
+    tap_reach = TAPS - 1
+    ids_bf = jnp.broadcast_to(doc_ids[tok_dev - tap_reach :, None], (tap_reach, 128)).astype(jnp.bfloat16)
+    packed = jnp.concatenate([gate_c[tok_dev - tap_reach :], value[tok_dev - tap_reach :], ids_bf], axis=1)
+    return passed_along(packed, "sp", 1)
 
 
 def mixer_rows(gate_b, gate_c, value, taps, doc_ids):
     tok_dev, width = gate_b.shape
     tap_reach = TAPS - 1
-    ids_bf = jnp.broadcast_to(doc_ids[tok_dev - tap_reach :, None], (tap_reach, 128)).astype(jnp.bfloat16)
-    packed = jnp.concatenate([gate_c[tok_dev - tap_reach :], value[tok_dev - tap_reach :], ids_bf], axis=1)
-    got = passed_along(packed, "sp", 1).astype(jnp.float32)
+    got = tail_passed(gate_c, value, doc_ids).astype(jnp.float32)
     prev_rows = got[:, :width] * got[:, width : 2 * width]
     id_values = doc_ids.astype(jnp.float32)
     ext_ids = jnp.concatenate([got[:, 2 * width], id_values], axis=0)

time: 213 us -> 219 us (1.028)
  the two profiles are of different devices: /device:TPU:11 before, /device:TPU:0 now
where the time goes in v4:
time: 219 us; the launch traced here: 218 us
  Pallas kernels  74.9 us (34%)
  starting transfers between devices  65.2 us (30%)
  waiting for transfers between devices  63.4 us (29%)
  matrix products  6.81 us (3%)
  local copies, waits for them, and re-layouts  3.85 us (2%)
  other arithmetic  3.81 us (2%)
    pallas_call x3, Pallas kernels, expert_blocks(): pl.pallas_call(functools.partial(expert_body, len(blocks)), grid=(units /...  65.9 us
    ppermute x30, waiting for transfers between devices, crossed(): lax.ppermute(block, 'sp', [(i, i ^ partner) for i in range(lax.axis_size(...  63.4 us
    ppermute x30, starting transfers between devices, crossed(): lax.ppermute(block, 'sp', [(i, i ^ partner) for i in range(lax.axis_size(...  62.8 us
    dot_general x1, matrix products, per_device(): jnp.dot(mixed, out_weight, preferred_element_type=jnp.float32)  6.81 us
    pallas_call x2, Pallas kernels, join_call(): pl.pallas_call(functools.partial(body, partners, first), out_shape=out, s...  6.21 us
  transfers between devices with their start and end apart: 31, of which 8 were waited for; matrix products, arithmetic and copies ran while one was open for 1% of the time, Pallas kernels for 32%

profile of v4, /device:TPU:0, one launch (start us, length us, event | category | flops | bytes accessed | tf_op | source)
XLA Modules:
  0.0 218.2 jit_solution(983963150662174508)
XLA Ops:
  2.5 2.4 %collective-permute-start = (bf16[2,4224]{1,0:T(2,128)(2,1)S(1)}, bf16[2,4224]{1,0:T(2,128)(2,1)S(1)}, u32[]{:S(2)}, u32[]{:S(2)}) collective-permute-start(bf16[2,4224]{1,0:T(2,128)(2,1)S(1)} %pad_maximum_fusion.1), channel_id=1, source_target_pairs={{0,1},{1,2},{2,3},{3,4},{4,5},{5,6},{6,7},{7,8},{8,9},{9,10},{10,1... | collective-permute-start | bytes 50696 | tf_op jit(solution)/shard_map/ppermute | solution.py:24
  4.9 1.9 convert_multiply_fusion.2
  7.5 6.8 %fusion.7 = (f32[256]{0:T(256)S(1)}, bf16[256,2048]{1,0:T(8,128)(2,1)S(1)}) fusion(bf16[2048,2048]{1,0:T(8,128)(2,1)} %param.19, f32[2,2048]{1,0:T(2,128)S(1)} %slice_multiply_fusion, f32[256,2048]{1,0:T(8,128)S(1)} %convert_multiply_fusion.2, bf16[256,2048]{1,0:T(8,128)(2,1)} %param.14, f32[2048]{0:T(1024)S(1)} %bitcast.12, f32[2048]{0:T(1024)S(1)} %bitcast.11, ...), kind=kOutput, calls=%fused_computation.12 | convolution fusion | flops 2155872000 | bytes 12625408 | tf_op jit(solution)/shard_map/dot_general | solution.py:337
  15.3 2.7 %pick.1 = (bf16[48,2048]{1,0:T(8,128)(2,1)}, bf16[48,2048]{1,0:T(8,128)(2,1)}, bf16[48,2048]{1,0:T(8,128)(2,1)}, bf16[48,2048]{1,0:T(8,128)(2,1)}, bf16[48,2048]...) custom-call(s32[2,256]{1,0:T(2,128)S(1)} %copy.15.routes_ref, ...), custom_call_target="tpu_custom_call" | custom-call | tf_op jit(solution)/shard_map/pick/pallas_call | solution.py:112
  18.0 2.7 %collective-permute-start.1 = (bf16[48,2048]{1,0:T(8,128)(2,1)}, bf16[48,2048]{1,0:T(8,128)(2,1)S(1)}, u32[]{:S(2)}, u32[]{:S(2)}) collective-permute-start(bf16[48,2048]{1,0:T(8,128)(2,1)} %get-tuple-element.38), channel_id=1, source_target_pairs={{0,1},{1,0},{2,3},{3,2},{4,5},{5,4},{6,7},{7,6},{8,9},{9,8},{10,11... | collective-permute-start | bytes 589832 | tf_op jit(solution)/shard_map/ppermute | solution.py:246
  20.6 1.5 collective-permute-start.2
  22.2 2.0 collective-permute-start.7
  24.2 2.5 %collective-permute-start.9 = (bf16[48,2048]{1,0:T(8,128)(2,1)}, bf16[48,2048]{1,0:T(8,128)(2,1)S(1)}, u32[]{:S(2)}, u32[]{:S(2)}) collective-permute-start(bf16[48,2048]{1,0:T(8,128)(2,1)} %get-tuple-element.47), channel_id=1, source_target_pairs={{0,6},{1,7},{2,4},{3,5},{4,2},{5,3},{6,0},{7,1},{8,14},{9,15},{10,... | collective-permute-start | bytes 589832 | tf_op jit(solution)/shard_map/ppermute | solution.py:246
  26.7 1.9 collective-permute-done.2.refs_2_
  29.1 2.0 collective-permute-done.3.refs_3_
  31.1 4.4 %collective-permute-start.11 = (bf16[48,2048]{1,0:T(8,128)(2,1)}, bf16[48,2048]{1,0:T(8,128)(2,1)S(1)}, u32[]{:S(2)}, u32[]{:S(2)}) collective-permute-start(bf16[48,2048]{1,0:T(8,128)(2,1)} %get-tuple-element.49), channel_id=1, source_target_pairs={{0,12},{1,13},{2,14},{3,15},{4,8},{5,9},{6,10},{7,11},{8,4},{9,5},... | collective-permute-start | bytes 589832 | tf_op jit(solution)/shard_map/ppermute | solution.py:246
  35.8 3.6 %collective-permute-start.13 = (bf16[48,2048]{1,0:T(8,128)(2,1)}, bf16[48,2048]{1,0:T(8,128)(2,1)S(1)}, u32[]{:S(2)}, u32[]{:S(2)}) collective-permute-start(bf16[48,2048]{1,0:T(8,128)(2,1)} %get-tuple-element.51), channel_id=1, source_target_pairs={{0,14},{1,15},{2,12},{3,13},{4,10},{5,11},{6,8},{7,9},{8,6},{9,7},... | collective-permute-start | bytes 589832 | tf_op jit(solution)/shard_map/ppermute | solution.py:246
  39.5 2.6 %collective-permute-start.14 = (bf16[48,2048]{1,0:T(8,128)(2,1)}, bf16[48,2048]{1,0:T(8,128)(2,1)S(1)}, u32[]{:S(2)}, u32[]{:S(2)}) collective-permute-start(bf16[48,2048]{1,0:T(8,128)(2,1)} %get-tuple-element.52), channel_id=1, source_target_pairs={{0,15},{1,14},{2,13},{3,12},{4,11},{5,10},{6,9},{7,8},{8,7},{9,6},... | collective-permute-start | bytes 589832 | tf_op jit(solution)/shard_map/ppermute | solution.py:246
  43.0 19.2 %experts.3 = (bf16[48,2048]{1,0:T(8,128)(2,1)S(1)}, bf16[48,2048]{1,0:T(8,128)(2,1)S(1)}, bf16[48,2048]{1,0:T(8,128)(2,1)S(1)}, bf16[48,2048]{1,0:T(8,128)(2,1)S(1)}) custom-call(bf16[48,2048]{1,0:T(8,128)(2,1)S(1)} %copy-done, bf16[48,2048]{1,0:T(8,128)(2,1)S(1)} %collective-permute-done.1.refs_1_, bf16[48,2048]{1,0:T(8,128)(2,1)S(1)} %collective-permute-done.2.refs_2_, ...), custom_call_target="tpu_custom_call" | custom-call | flops 9663676416 | bytes 51904512 | tf_op jit(solution)/shard_map/experts/pallas_call | solution.py:216
  62.3 3.8 %collective-permute-start.20 = (bf16[48,2048]{1,0:T(8,128)(2,1)S(1)}, bf16[48,2048]{1,0:T(8,128)(2,1)S(1)}, u32[]{:S(2)}, u32[]{:S(2)}) collective-permute-start(bf16[48,2048]{1,0:T(8,128)(2,1)S(1)} %copy-done.14), channel_id=1, source_target_pairs={{0,9},{1,8},{2,11},{3,10},{4,13},{5,12},{6,15},{7,14},{8,1},{9,0},... | collective-permute-start | bytes 589832 | tf_op jit(solution)/shard_map/ppermute | solution.py:246
  66.5 13.9 %collective-permute-start.22 = (bf16[48,2048]{1,0:T(8,128)(2,1)S(1)}, bf16[48,2048]{1,0:T(8,128)(2,1)S(1)}, u32[]{:S(2)}, u32[]{:S(2)}) collective-permute-start(bf16[48,2048]{1,0:T(8,128)(2,1)S(1)} %copy-done.12), channel_id=1, source_target_pairs={{0,11},{1,10},{2,9},{3,8},{4,15},{5,14},{6,13},{7,12},{8,3},{9,2},... | collective-permute-start | bytes 589832 | tf_op jit(solution)/shard_map/ppermute | solution.py:246
  80.5 1.0 collective-permute-start.4
  81.5 27.1 %experts.4 = (bf16[48,2048]{1,0:T(8,128)(2,1)S(1)}, bf16[48,2048]{1,0:T(8,128)(2,1)S(1)}, bf16[48,2048]{1,0:T(8,128)(2,1)}, bf16[48,2048]{1,0:T(8,128)(2,1)}, bf...) custom-call(bf16[48,2048]{1,0:T(8,128)(2,1)S(1)} %collective-permute, ...), custom_call_target="tpu_custom_call" | custom-call | flops 19327352832 | bytes 53477376 | tf_op jit(solution)/shard_map/experts/pallas_call | solution.py:216
  110.0 7.0 %collective-permute-start.15 = (bf16[48,2048]{1,0:T(8,128)(2,1)S(1)}, bf16[48,2048]{1,0:T(8,128)(2,1)S(1)}, u32[]{:S(2)}, u32[]{:S(2)}) collective-permute-start(bf16[48,2048]{1,0:T(8,128)(2,1)S(1)} %get-tuple-element.53), channel_id=1, source_target_pairs={{0,4},{1,5},{2,6},{3,7},{4,0},{5,1},{6,2},{7,3},{8,12},{9,13},{10,... | collective-permute-start | bytes 589832 | tf_op jit(solution)/shard_map/ppermute | solution.py:246
  117.0 19.7 %experts.5 = (bf16[48,2048]{1,0:T(8,128)(2,1)}, bf16[48,2048]{1,0:T(8,128)(2,1)}, bf16[48,2048]{1,0:T(8,128)(2,1)}, bf16[48,2048]{1,0:T(8,128)(2,1)S(1)}) custom-call(bf16[48,2048]{1,0:T(8,128)(2,1)S(1)} %collective-permute-done.19.refs_0_, bf16[48,2048]{1,0:T(8,128)(2,1)S(1)} %collective-permute-done.20.refs_1_, ...), custom_call_target="tpu_custom_call" | custom-call | flops 9663676416 | bytes 51904512 | tf_op jit(solution)/shard_map/experts/pallas_call | solution.py:216
  137.5 2.2 %collective-permute-start.17 = (bf16[48,2048]{1,0:T(8,128)(2,1)}, bf16[48,2048]{1,0:T(8,128)(2,1)}, u32[]{:S(2)}, u32[]{:S(2)}) collective-permute-start(bf16[48,2048]{1,0:T(8,128)(2,1)} %get-tuple-element.55), channel_id=1, source_target_pairs={{0,6},{1,7},{2,4},{3,5},{4,2},{5,3},{6,0},{7,1},{8,14},{9,15},{10,... | collective-permute-start | bytes 589832 | tf_op jit(solution)/shard_map/ppermute | solution.py:246
  140.7 2.1 collective-permute-start.24
  143.8 7.9 %collective-permute-done.17.refs_6_ = bf16[48,2048]{1,0:T(8,128)(2,1)} collective-permute-done((bf16[48,2048]{1,0:T(8,128)(2,1)}, bf16[48,2048]{1,0:T(8,128)(2,1)}, u32[]{:S(2)}, u32[]{:S(2)}) %collective-permute-start.17) | collective-permute-done | bytes 196640 | tf_op jit(solution)/shard_map/ppermute | solution.py:246
  151.7 2.5 %collective-permute-start.27 = (bf16[48,2048]{1,0:T(8,128)(2,1)}, bf16[48,2048]{1,0:T(8,128)(2,1)S(1)}, u32[]{:S(2)}, u32[]{:S(2)}) collective-permute-start(bf16[48,2048]{1,0:T(8,128)(2,1)} %copy-done.4), channel_id=1, source_target_pairs={{0,12},{1,13},{2,14},{3,15},{4,8},{5,9},{6,10},{7,11},{8,4},{9,5},... | collective-permute-start | bytes 589832 | tf_op jit(solution)/shard_map/ppermute | solution.py:246
  154.3 3.1 %collective-permute-start.28 = (bf16[48,2048]{1,0:T(8,128)(2,1)}, bf16[48,2048]{1,0:T(8,128)(2,1)S(1)}, u32[]{:S(2)}, u32[]{:S(2)}) collective-permute-start(bf16[48,2048]{1,0:T(8,128)(2,1)} %copy-done.3), channel_id=1, source_target_pairs={{0,13},{1,12},{2,15},{3,14},{4,9},{5,8},{6,11},{7,10},{8,5},{9,4},... | collective-permute-start | bytes 589832 | tf_op jit(solution)/shard_map/ppermute | solution.py:246
  157.4 1.4 collective-permute-start.29
  158.8 18.9 %collective-permute-done.24.refs_9_ = bf16[48,2048]{1,0:T(8,128)(2,1)} collective-permute-done((bf16[48,2048]{1,0:T(8,128)(2,1)}, bf16[48,2048]{1,0:T(8,128)(2,1)}, u32[]{:S(2)}, u32[]{:S(2)}) %collective-permute-start.24) | collective-permute-done | bytes 196640 | tf_op jit(solution)/shard_map/ppermute | solution.py:246
  177.7 1.8 collective-permute-start.30
  179.5 3.5 %collective-permute-done.25.refs_10_ = bf16[48,2048]{1,0:T(8,128)(2,1)} collective-permute-done((bf16[48,2048]{1,0:T(8,128)(2,1)}, bf16[48,2048]{1,0:T(8,128)(2,1)}, u32[]{:S(2)}, u32[]{:S(2)}) %collective-permute-start.25) | collective-permute-done | bytes 196640 | tf_op jit(solution)/shard_map/ppermute | solution.py:246
  183.1 28.9 %collective-permute-done.26.refs_11_ = bf16[48,2048]{1,0:T(8,128)(2,1)S(1)} collective-permute-done((bf16[48,2048]{1,0:T(8,128)(2,1)}, bf16[48,2048]{1,0:T(8,128)(2,1)S(1)}, u32[]{:S(2)}, u32[]{:S(2)}) %collective-permute-start.26) | collective-permute-done | bytes 196640 | tf_op jit(solution)/shard_map/ppermute | solution.py:246
  212.0 3.7 %shard_map.127.part_ref = f32[256,2048]{1,0:T(8,128)S(1)} custom-call(s32[256,2]{1,0:T(8,128)S(1)} %broadcast_xor_fusion.partner_ref, f32[256,2]{1,0:T(8,128)S(1)} %copy.17.share_ref, bf16[48,2048]{1,0:T(8,128)(2,1)S(1)} %get-tuple-element.41.refs_0_, bf16[48,2048]{1,0:T(8,128)(2,1)S(1)} %collective-permute-done.4.refs_1_, ...), custom_call_target="tpu_custom_call" | custom-call | tf_op jit(solution)/shard_map/pallas_call | solution.py:171
  215.7 2.5 %shard_map.128 = bf16[256,2048]{1,0:T(8,128)(2,1)} custom-call(s32[256,2]{1,0:T(8,128)S(1)} %broadcast_xor_fusion.partner_ref, f32[256,2]{1,0:T(8,128)S(1)} %copy.17.share_ref, f32[1,2048]{1,0:T(1,128)S(1)} %get-tuple-element.72.gain_ref, f32[256,2048]{1,0:T(8,128)S(1)} %get-tuple-element.70.stream_ref, f32[256,2048]{1,0:T(8,128)S(1)} %shard_map.127.part_ref, ...), custom_call_target="tpu_custom_call" | custom-call | tf_op jit(solution)/shard_map/pallas_call | solution.py:171
  (92 shorter events, 10.5 us)
Async XLA Ops:
  2.5 4.7 %collective-permute-start = (bf16[2,4224]{1,0:T(2,128)(2,1)S(1)}, bf16[2,4224]{1,0:T(2,128)(2,1)S(1)}, u32[]{:S(2)}, u32[]{:S(2)}) collective-permute-start(bf16[2,4224]{1,0:T(2,128)(2,1)S(1)} %pad_maximum_fusion.1), channel_id=1, source_target_pairs={{0,1},{1,2},{2,3},{3,4},{4,5},{5,6},{6,7},{7,8},{8,9},{9,10},{10,1... | collective-permute-start | bytes 50696 | tf_op jit(solution)/shard_map/ppermute | solution.py:24
  18.0 6.2 %collective-permute-start.1 = (bf16[48,2048]{1,0:T(8,128)(2,1)}, bf16[48,2048]{1,0:T(8,128)(2,1)S(1)}, u32[]{:S(2)}, u32[]{:S(2)}) collective-permute-start(bf16[48,2048]{1,0:T(8,128)(2,1)} %get-tuple-element.38), channel_id=1, source_target_pairs={{0,1},{1,0},{2,3},{3,2},{4,5},{5,4},{6,7},{7,6},{8,9},{9,8},{10,11... | collective-permute-start | bytes 589832 | tf_op jit(solution)/shard_map/ppermute | solution.py:246
  20.6 8.0 %collective-permute-start.2 = (bf16[48,2048]{1,0:T(8,128)(2,1)}, bf16[48,2048]{1,0:T(8,128)(2,1)S(1)}, u32[]{:S(2)}, u32[]{:S(2)}) collective-permute-start(bf16[48,2048]{1,0:T(8,128)(2,1)} %get-tuple-element.39), channel_id=1, source_target_pairs={{0,2},{1,3},{2,0},{3,1},{4,6},{5,7},{6,4},{7,5},{8,10},{9,11},{10,... | collective-permute-start | bytes 589832 | tf_op jit(solution)/shard_map/ppermute | solution.py:246
  22.2 8.9 %collective-permute-start.3 = (bf16[48,2048]{1,0:T(8,128)(2,1)}, bf16[48,2048]{1,0:T(8,128)(2,1)S(1)}, u32[]{:S(2)}, u32[]{:S(2)}) collective-permute-start(bf16[48,2048]{1,0:T(8,128)(2,1)} %get-tuple-element.40), channel_id=1, source_target_pairs={{0,3},{1,2},{2,1},{3,0},{4,7},{5,6},{6,5},{7,4},{8,11},{9,10},{10,... | collective-permute-start | bytes 589832 | tf_op jit(solution)/shard_map/ppermute | solution.py:246
  22.2 13.4 %collective-permute-start.7 = (bf16[48,2048]{1,0:T(8,128)(2,1)}, bf16[48,2048]{1,0:T(8,128)(2,1)S(1)}, u32[]{:S(2)}, u32[]{:S(2)}) collective-permute-start(bf16[48,2048]{1,0:T(8,128)(2,1)} %get-tuple-element.45), channel_id=1, source_target_pairs={{0,4},{1,5},{2,6},{3,7},{4,0},{5,1},{6,2},{7,3},{8,12},{9,13},{10,... | collective-permute-start | bytes 589832 | tf_op jit(solution)/shard_map/ppermute | solution.py:246
  24.2 11.6 %collective-permute-start.8 = (bf16[48,2048]{1,0:T(8,128)(2,1)}, bf16[48,2048]{1,0:T(8,128)(2,1)S(1)}, u32[]{:S(2)}, u32[]{:S(2)}) collective-permute-start(bf16[48,2048]{1,0:T(8,128)(2,1)} %get-tuple-element.46), channel_id=1, source_target_pairs={{0,5},{1,4},{2,7},{3,6},{4,1},{5,0},{6,3},{7,2},{8,13},{9,12},{10,... | collective-permute-start | bytes 589832 | tf_op jit(solution)/shard_map/ppermute | solution.py:246
  24.2 15.3 %collective-permute-start.9 = (bf16[48,2048]{1,0:T(8,128)(2,1)}, bf16[48,2048]{1,0:T(8,128)(2,1)S(1)}, u32[]{:S(2)}, u32[]{:S(2)}) collective-permute-start(bf16[48,2048]{1,0:T(8,128)(2,1)} %get-tuple-element.47), channel_id=1, source_target_pairs={{0,6},{1,7},{2,4},{3,5},{4,2},{5,3},{6,0},{7,1},{8,14},{9,15},{10,... | collective-permute-start | bytes 589832 | tf_op jit(solution)/shard_map/ppermute | solution.py:246
  28.6 33.5 %collective-permute-start.10 = (bf16[48,2048]{1,0:T(8,128)(2,1)}, bf16[48,2048]{1,0:T(8,128)(2,1)S(1)}, u32[]{:S(2)}, u32[]{:S(2)}) collective-permute-start(bf16[48,2048]{1,0:T(8,128)(2,1)} %get-tuple-element.48), channel_id=1, source_target_pairs={{0,7},{1,6},{2,5},{3,4},{4,3},{5,2},{6,1},{7,0},{8,15},{9,14},{10,... | collective-permute-start | bytes 589832 | tf_op jit(solution)/shard_map/ppermute | solution.py:246
  31.1 31.1 %collective-permute-start.11 = (bf16[48,2048]{1,0:T(8,128)(2,1)}, bf16[48,2048]{1,0:T(8,128)(2,1)S(1)}, u32[]{:S(2)}, u32[]{:S(2)}) collective-permute-start(bf16[48,2048]{1,0:T(8,128)(2,1)} %get-tuple-element.49), channel_id=1, source_target_pairs={{0,12},{1,13},{2,14},{3,15},{4,8},{5,9},{6,10},{7,11},{8,4},{9,5},... | collective-permute-start | bytes 589832 | tf_op jit(solution)/shard_map/ppermute | solution.py:246
  35.6 30.5 %collective-permute-start.12 = (bf16[48,2048]{1,0:T(8,128)(2,1)}, bf16[48,2048]{1,0:T(8,128)(2,1)S(1)}, u32[]{:S(2)}, u32[]{:S(2)}) collective-permute-start(bf16[48,2048]{1,0:T(8,128)(2,1)} %get-tuple-element.50), channel_id=1, source_target_pairs={{0,13},{1,12},{2,15},{3,14},{4,9},{5,8},{6,11},{7,10},{8,5},{9,4},... | collective-permute-start | bytes 589832 | tf_op jit(solution)/shard_map/ppermute | solution.py:246
  35.8 30.7 %collective-permute-start.13 = (bf16[48,2048]{1,0:T(8,128)(2,1)}, bf16[48,2048]{1,0:T(8,128)(2,1)S(1)}, u32[]{:S(2)}, u32[]{:S(2)}) collective-permute-start(bf16[48,2048]{1,0:T(8,128)(2,1)} %get-tuple-element.51), channel_id=1, source_target_pairs={{0,14},{1,15},{2,12},{3,13},{4,10},{5,11},{6,8},{7,9},{8,6},{9,7},... | collective-permute-start | bytes 589832 | tf_op jit(solution)/shard_map/ppermute | solution.py:246
  39.5 41.0 %collective-permute-start.14 = (bf16[48,2048]{1,0:T(8,128)(2,1)}, bf16[48,2048]{1,0:T(8,128)(2,1)S(1)}, u32[]{:S(2)}, u32[]{:S(2)}) collective-permute-start(bf16[48,2048]{1,0:T(8,128)(2,1)} %get-tuple-element.52), channel_id=1, source_target_pairs={{0,15},{1,14},{2,13},{3,12},{4,11},{5,10},{6,9},{7,8},{8,7},{9,6},... | collective-permute-start | bytes 589832 | tf_op jit(solution)/shard_map/ppermute | solution.py:246
  62.2 46.4 %collective-permute-start.19 = (bf16[48,2048]{1,0:T(8,128)(2,1)S(1)}, bf16[48,2048]{1,0:T(8,128)(2,1)S(1)}, u32[]{:S(2)}, u32[]{:S(2)}) collective-permute-start(bf16[48,2048]{1,0:T(8,128)(2,1)S(1)} %copy-done.15), channel_id=1, source_target_pairs={{0,8},{1,9},{2,10},{3,11},{4,12},{5,13},{6,14},{7,15},{8,0},{9,1},... | collective-permute-start | bytes 589832 | tf_op jit(solution)/shard_map/ppermute | solution.py:246
  62.3 47.0 %collective-permute-start.20 = (bf16[48,2048]{1,0:T(8,128)(2,1)S(1)}, bf16[48,2048]{1,0:T(8,128)(2,1)S(1)}, u32[]{:S(2)}, u32[]{:S(2)}) collective-permute-start(bf16[48,2048]{1,0:T(8,128)(2,1)S(1)} %copy-done.14), channel_id=1, source_target_pairs={{0,9},{1,8},{2,11},{3,10},{4,13},{5,12},{6,15},{7,14},{8,1},{9,0},... | collective-permute-start | bytes 589832 | tf_op jit(solution)/shard_map/ppermute | solution.py:246
  66.1 43.9 %collective-permute-start.21 = (bf16[48,2048]{1,0:T(8,128)(2,1)S(1)}, bf16[48,2048]{1,0:T(8,128)(2,1)S(1)}, u32[]{:S(2)}, u32[]{:S(2)}) collective-permute-start(bf16[48,2048]{1,0:T(8,128)(2,1)S(1)} %copy-done.13), channel_id=1, source_target_pairs={{0,10},{1,11},{2,8},{3,9},{4,14},{5,15},{6,12},{7,13},{8,2},{9,3},... | collective-permute-start | bytes 589832 | tf_op jit(solution)/shard_map/ppermute | solution.py:246
  66.5 50.5 %collective-permute-start.22 = (bf16[48,2048]{1,0:T(8,128)(2,1)S(1)}, bf16[48,2048]{1,0:T(8,128)(2,1)S(1)}, u32[]{:S(2)}, u32[]{:S(2)}) collective-permute-start(bf16[48,2048]{1,0:T(8,128)(2,1)S(1)} %copy-done.12), channel_id=1, source_target_pairs={{0,11},{1,10},{2,9},{3,8},{4,15},{5,14},{6,13},{7,12},{8,3},{9,2},... | collective-permute-start | bytes 589832 | tf_op jit(solution)/shard_map/ppermute | solution.py:246
  80.5 57.0 %collective-permute-start.4 = (bf16[48,2048]{1,0:T(8,128)(2,1)S(1)}, bf16[48,2048]{1,0:T(8,128)(2,1)S(1)}, u32[]{:S(2)}, u32[]{:S(2)}) collective-permute-start(bf16[48,2048]{1,0:T(8,128)(2,1)S(1)} %get-tuple-element.42), channel_id=1, source_target_pairs={{0,1},{1,0},{2,3},{3,2},{4,5},{5,4},{6,7},{7,6},{8,9},{9,8},{10,11... | collective-permute-start | bytes 589832 | tf_op jit(solution)/shard_map/ppermute | solution.py:246
  108.6 28.2 %copy-start.4 = (bf16[48,2048]{1,0:T(8,128)(2,1)}, bf16[48,2048]{1,0:T(8,128)(2,1)S(1)}, u32[]{:S(2)}) copy-start(bf16[48,2048]{1,0:T(8,128)(2,1)S(1)} %get-tuple-element.65) | copy-start | bytes 589828
  108.6 31.1 %collective-permute-start.5 = (bf16[48,2048]{1,0:T(8,128)(2,1)S(1)}, bf16[48,2048]{1,0:T(8,128)(2,1)S(1)}, u32[]{:S(2)}, u32[]{:S(2)}) collective-permute-start(bf16[48,2048]{1,0:T(8,128)(2,1)S(1)} %get-tuple-element.43), channel_id=1, source_target_pairs={{0,2},{1,3},{2,0},{3,1},{4,6},{5,7},{6,4},{7,5},{8,10},{9,11},{10,... | collective-permute-start | bytes 589832 | tf_op jit(solution)/shard_map/ppermute | solution.py:246
  109.3 30.6 %collective-permute-start.6 = (bf16[48,2048]{1,0:T(8,128)(2,1)S(1)}, bf16[48,2048]{1,0:T(8,128)(2,1)S(1)}, u32[]{:S(2)}, u32[]{:S(2)}) collective-permute-start(bf16[48,2048]{1,0:T(8,128)(2,1)S(1)} %get-tuple-element.44), channel_id=1, source_target_pairs={{0,3},{1,2},{2,1},{3,0},{4,7},{5,6},{6,5},{7,4},{8,11},{9,10},{10,... | collective-permute-start | bytes 589832 | tf_op jit(solution)/shard_map/ppermute | solution.py:246
  110.0 30.6 %collective-permute-start.15 = (bf16[48,2048]{1,0:T(8,128)(2,1)S(1)}, bf16[48,2048]{1,0:T(8,128)(2,1)S(1)}, u32[]{:S(2)}, u32[]{:S(2)}) collective-permute-start(bf16[48,2048]{1,0:T(8,128)(2,1)S(1)} %get-tuple-element.53), channel_id=1, source_target_pairs={{0,4},{1,5},{2,6},{3,7},{4,0},{5,1},{6,2},{7,3},{8,12},{9,13},{10,... | collective-permute-start | bytes 589832 | tf_op jit(solution)/shard_map/ppermute | solution.py:246
  117.0 25.7 %collective-permute-start.16 = (bf16[48,2048]{1,0:T(8,128)(2,1)S(1)}, bf16[48,2048]{1,0:T(8,128)(2,1)S(1)}, u32[]{:S(2)}, u32[]{:S(2)}) collective-permute-start(bf16[48,2048]{1,0:T(8,128)(2,1)S(1)} %get-tuple-element.54), channel_id=1, source_target_pairs={{0,5},{1,4},{2,7},{3,6},{4,1},{5,0},{6,3},{7,2},{8,13},{9,12},{10,... | collective-permute-start | bytes 589832 | tf_op jit(solution)/shard_map/ppermute | solution.py:246
  137.5 14.3 %collective-permute-start.17 = (bf16[48,2048]{1,0:T(8,128)(2,1)}, bf16[48,2048]{1,0:T(8,128)(2,1)}, u32[]{:S(2)}, u32[]{:S(2)}) collective-permute-start(bf16[48,2048]{1,0:T(8,128)(2,1)} %get-tuple-element.55), channel_id=1, source_target_pairs={{0,6},{1,7},{2,4},{3,5},{4,2},{5,3},{6,0},{7,1},{8,14},{9,15},{10,... | collective-permute-start | bytes 589832 | tf_op jit(solution)/shard_map/ppermute | solution.py:246
  139.7 14.6 %collective-permute-start.18 = (bf16[48,2048]{1,0:T(8,128)(2,1)}, bf16[48,2048]{1,0:T(8,128)(2,1)}, u32[]{:S(2)}, u32[]{:S(2)}) collective-permute-start(bf16[48,2048]{1,0:T(8,128)(2,1)} %get-tuple-element.56), channel_id=1, source_target_pairs={{0,7},{1,6},{2,5},{3,4},{4,3},{5,2},{6,1},{7,0},{8,15},{9,14},{10,... | collective-permute-start | bytes 589832 | tf_op jit(solution)/shard_map/ppermute | solution.py:246
  139.9 17.5 %collective-permute-start.23 = (bf16[48,2048]{1,0:T(8,128)(2,1)}, bf16[48,2048]{1,0:T(8,128)(2,1)}, u32[]{:S(2)}, u32[]{:S(2)}) collective-permute-start(bf16[48,2048]{1,0:T(8,128)(2,1)} %get-tuple-element.61), channel_id=1, source_target_pairs={{0,8},{1,9},{2,10},{3,11},{4,12},{5,13},{6,14},{7,15},{8,0},{9,1},... | collective-permute-start | bytes 589832 | tf_op jit(solution)/shard_map/ppermute | solution.py:246
  140.7 37.1 %collective-permute-start.24 = (bf16[48,2048]{1,0:T(8,128)(2,1)}, bf16[48,2048]{1,0:T(8,128)(2,1)}, u32[]{:S(2)}, u32[]{:S(2)}) collective-permute-start(bf16[48,2048]{1,0:T(8,128)(2,1)} %get-tuple-element.62), channel_id=1, source_target_pairs={{0,9},{1,8},{2,11},{3,10},{4,13},{5,12},{6,15},{7,14},{8,1},{9,0},... | collective-permute-start | bytes 589832 | tf_op jit(solution)/shard_map/ppermute | solution.py:246
  142.8 40.3 %collective-permute-start.25 = (bf16[48,2048]{1,0:T(8,128)(2,1)}, bf16[48,2048]{1,0:T(8,128)(2,1)}, u32[]{:S(2)}, u32[]{:S(2)}) collective-permute-start(bf16[48,2048]{1,0:T(8,128)(2,1)} %get-tuple-element.63), channel_id=1, source_target_pairs={{0,10},{1,11},{2,8},{3,9},{4,14},{5,15},{6,12},{7,13},{8,2},{9,3},... | collective-permute-start | bytes 589832 | tf_op jit(solution)/shard_map/ppermute | solution.py:246
  151.7 63.9 %collective-permute-start.27 = (bf16[48,2048]{1,0:T(8,128)(2,1)}, bf16[48,2048]{1,0:T(8,128)(2,1)S(1)}, u32[]{:S(2)}, u32[]{:S(2)}) collective-permute-start(bf16[48,2048]{1,0:T(8,128)(2,1)} %copy-done.4), channel_id=1, source_target_pairs={{0,12},{1,13},{2,14},{3,15},{4,8},{5,9},{6,10},{7,11},{8,4},{9,5},... | collective-permute-start | bytes 589832 | tf_op jit(solution)/shard_map/ppermute | solution.py:246
  154.3 61.3 %collective-permute-start.28 = (bf16[48,2048]{1,0:T(8,128)(2,1)}, bf16[48,2048]{1,0:T(8,128)(2,1)S(1)}, u32[]{:S(2)}, u32[]{:S(2)}) collective-permute-start(bf16[48,2048]{1,0:T(8,128)(2,1)} %copy-done.3), channel_id=1, source_target_pairs={{0,13},{1,12},{2,15},{3,14},{4,9},{5,8},{6,11},{7,10},{8,5},{9,4},... | collective-permute-start | bytes 589832 | tf_op jit(solution)/shard_map/ppermute | solution.py:246
  157.4 58.3 %collective-permute-start.29 = (bf16[48,2048]{1,0:T(8,128)(2,1)}, bf16[48,2048]{1,0:T(8,128)(2,1)S(1)}, u32[]{:S(2)}, u32[]{:S(2)}) collective-permute-start(bf16[48,2048]{1,0:T(8,128)(2,1)} %copy-done.2), channel_id=1, source_target_pairs={{0,14},{1,15},{2,12},{3,13},{4,10},{5,11},{6,8},{7,9},{8,6},{9,7},... | collective-permute-start | bytes 589832 | tf_op jit(solution)/shard_map/ppermute | solution.py:246
  177.7 38.0 %collective-permute-start.30 = (bf16[48,2048]{1,0:T(8,128)(2,1)}, bf16[48,2048]{1,0:T(8,128)(2,1)S(1)}, u32[]{:S(2)}, u32[]{:S(2)}) collective-permute-start(bf16[48,2048]{1,0:T(8,128)(2,1)} %copy-done.1), channel_id=1, source_target_pairs={{0,15},{1,14},{2,13},{3,12},{4,11},{5,10},{6,9},{7,8},{8,7},{9,6},... | collective-permute-start | bytes 589832 | tf_op jit(solution)/shard_map/ppermute | solution.py:246
  183.1 28.9 %collective-permute-start.26 = (bf16[48,2048]{1,0:T(8,128)(2,1)}, bf16[48,2048]{1,0:T(8,128)(2,1)S(1)}, u32[]{:S(2)}, u32[]{:S(2)}) collective-permute-start(bf16[48,2048]{1,0:T(8,128)(2,1)} %copy-done.5), channel_id=1, source_target_pairs={{0,11},{1,10},{2,9},{3,8},{4,15},{5,14},{6,13},{7,12},{8,3},{9,2},... | collective-permute-start | bytes 589832 | tf_op jit(solution)/shard_map/ppermute | solution.py:246
  (15 other events, 213.3 us)
